TPU v7x, 32 devices: a whole 2x2x4 slice. The times are simulated.
32 devices in a mesh: fs: 4 (over y, x), tp: 8 (over z, core).
Axes of the slice: x: 2, y: 2, z: 4, core: 2. Of those that a mesh axis runs over, the one named last changes fastest.
Arguments:
- prompt: bfloat16 [4096, 2048], P(('fs', 'tp')), may hold values from -6 to 6
- norm_gain: float32 [2048], P('tp'), may hold values from 0.1 to 1.9
- gate_master: float32 [8, 2, 512, 2048], P(None, None, 'fs', 'tp'), may hold values from -0.125 to 0.125
- up_master: float32 [8, 2, 512, 2048], P(None, None, 'fs', 'tp'), may hold values from -0.125 to 0.125
- down_master: float32 [8, 2, 512, 2048], P(None, None, 'fs', 'tp'), may hold values from -0.25 to 0.25
- group_pick: int32 [4096, 1], P(('fs', 'tp')), may hold values from 0 to 7; in each aligned block of 128 rows (0 to 127, 128 to 255, ...) at most 32 rows name the same one
- route_weight: bfloat16 [4096, 2], P(('fs', 'tp')), may hold values from 0.099609375 to 1
Outputs:
- gate_serve: bfloat16 [8, 2, 512, 2048], P('tp', None, 'fs')
- up_serve: bfloat16 [8, 2, 512, 2048], P('tp', None, 'fs')
- down_serve: bfloat16 [8, 2, 512, 2048], P('tp', None, 'fs')
- mixed: bfloat16 [4096, 2048], P(('fs', 'tp'))
Inputs may be any that keep to these rules, and one draw needn't show every extreme that they name: `group_pick`: in the rows of one device no group is named by more than 32 rows, and in every draw some device's rows name one group exactly 32 times.
All inputs are finite; a program needn't handle non-finite values.
Results may differ from a plain program's by a relative error of at most 0.0081.
Values may be sent and summed in bfloat16 or wider, within the bound.
No kernel may reach another device: no remote copies, remote signals or barrier semaphores. Data moves between devices by JAX's collectives and lax.ppermute only.
A program may use at most 64 MiB of HBM per device.

v0:
```python
import functools

import jax
import jax.numpy as jnp
from jax import lax
from jax.experimental import pallas as pl
from jax.experimental.pallas import tpu as pltpu
from jax.sharding import PartitionSpec as P


EPS = 1e-06
LANES = 128
VMEM = pl.BlockSpec(memory_space=pltpu.VMEM)


def nt_dot(left, right):
    return lax.dot_general(left, right, (((1,), (1,)), ((), ())), preferred_element_type=jnp.float32)


def cost(flops, moved):
    return pl.CostEstimate(flops=int(flops), bytes_accessed=int(moved), transcendentals=0)


def swap(value, axis, distance):
    count = lax.axis_size(axis)
    return lax.ppermute(value, axis, [(i, i ^ distance) for i in range(count)])


def far_first(count):
    half = count // 2
    return list(range(half, count)) + list(range(2, half)) + ([1] if half > 1 else [])


def route_kernel(cap, me_ref, prompt_ref, pick_ref, weight_ref, *out_refs):
    placing_ref, blocks = out_refs[0], out_refs[1:]
    slots, tokens = placing_ref.shape
    width = prompt_ref.shape[1]
    values = prompt_ref[...].astype(jnp.float32)
    scale = lax.rsqrt(jnp.mean(values * values, axis=1, keepdims=True) + EPS)
    normed = (values * scale).astype(jnp.bfloat16)
    distance = pick_ref[...] ^ me_ref[0]
    count = max(8, len(blocks))
    member = (lax.broadcasted_iota(jnp.int32, (count, tokens), 0) == distance).astype(jnp.float32)
    before = lax.broadcasted_iota(jnp.int32, (tokens, tokens), 0) < lax.broadcasted_iota(
        jnp.int32, (tokens, tokens), 1
    )
    earlier = jnp.dot(
        member.astype(jnp.bfloat16), before.astype(jnp.float32).astype(jnp.bfloat16),
        preferred_element_type=jnp.float32,
    )
    rank = jnp.sum(earlier * member, axis=0, keepdims=True).astype(jnp.int32)
    target = distance * cap + rank
    placing = (lax.broadcasted_iota(jnp.int32, (slots, tokens), 0) == target).astype(jnp.float32)
    placing = placing.astype(jnp.bfloat16)
    placing_ref[...] = placing
    weights = weight_ref[...].astype(jnp.float32)
    experts = weights.shape[0]
    row = lax.broadcasted_iota(jnp.int32, (LANES, tokens), 0)
    spread = jnp.zeros((LANES, tokens), jnp.float32)
    for x in range(experts):
        spread = jnp.where(row == x, weights[x : x + 1, :], spread)
    placed_weights = nt_dot(placing, spread.astype(jnp.bfloat16)).astype(jnp.bfloat16)
    rows = jnp.dot(placing, normed, preferred_element_type=jnp.float32).astype(jnp.bfloat16)
    for d, block in enumerate(blocks):
        block[:, :width] = rows[d * cap : (d + 1) * cap]
        block[:, width:] = placed_weights[d * cap : (d + 1) * cap]


def route(me, prompt, group_pick, route_weight):
    tokens, width = prompt.shape
    groups = lax.axis_size("tp")
    cap = 2 * tokens // groups
    block = jax.ShapeDtypeStruct((cap, width + LANES), jnp.bfloat16)
    outs = pl.pallas_call(
        functools.partial(route_kernel, cap),
        out_shape=[jax.ShapeDtypeStruct((groups * cap, tokens), jnp.bfloat16)] + [block] * groups,
        in_specs=[pl.BlockSpec(memory_space=pltpu.SMEM)] + [VMEM] * 3,
        out_specs=[VMEM] * (groups + 1),
        cost_estimate=cost(2 * groups * cap * tokens * width, 2 * tokens * width * 6),
        name="route",
    )(me, prompt, group_pick.reshape(1, tokens), route_weight.T)
    return outs[0], outs[1:]


def round_kernel(scaled, me_ref, gain_ref, master_ref, after_ref, *blocks):
    gain = gain_ref[...].reshape(1, 1, -1)
    for d, block in enumerate(blocks):
        values = master_ref[me_ref[0] ^ d]
        if scaled:
            values = values * gain
        block[...] = values.astype(jnp.bfloat16)


def rounded(me, gain, master, scaled, after):
    groups, experts, units, part = master.shape
    block = jax.ShapeDtypeStruct((experts, units, part), jnp.bfloat16)
    size = groups * experts * units * part
    return pl.pallas_call(
        functools.partial(round_kernel, scaled),
        out_shape=[block] * groups,
        in_specs=[pl.BlockSpec(memory_space=pltpu.SMEM)]
        + [VMEM] * 2
        + [pl.BlockSpec(memory_space=pl.ANY)],
        out_specs=[VMEM] * groups,
        cost_estimate=cost(4 * size, 6 * size),
        name="rounding",
    )(me, gain.reshape(1, -1), master, after)


def joined(me, blocks):
    count = len(blocks)
    experts, units, part = blocks[0].shape
    if part % LANES:
        order = jnp.stack(blocks)[me[0] ^ jnp.arange(count)]
        return jnp.moveaxis(order, 0, 2).reshape(1, experts, units, count * part)

    def kernel(me_ref, *refs):
        ins, out_ref, sems = refs[:count], refs[count], refs[count + 1]
        copies = []
        for d in range(count):
            start = pl.multiple_of((me_ref[0] ^ d) * part, part)
            copies.append(
                pltpu.make_async_copy(ins[d], out_ref.at[0, :, :, pl.ds(start, part)], sems.at[d])
            )
        for copy in copies:
            copy.start()
        for copy in copies:
            copy.wait()

    size = count * experts * units * part
    return pl.pallas_call(
        kernel,
        out_shape=jax.ShapeDtypeStruct((1, experts, units, count * part), jnp.bfloat16),
        in_specs=[pl.BlockSpec(memory_space=pltpu.SMEM)] + [VMEM] * count,
        out_specs=pl.BlockSpec(memory_space=pl.ANY),
        scratch_shapes=[pltpu.SemaphoreType.DMA((count,))],
        cost_estimate=cost(4 * size, 4 * size),
        name="joining",
    )(me, *blocks)


def stack_rows_kernel(width, *refs):
    blocks, rows_ref, weights_ref = refs[:-2], refs[-2], refs[-1]
    cap = blocks[0].shape[0]
    for d, block in enumerate(blocks):
        rows_ref[d * cap : (d + 1) * cap] = block[:, :width]
        weights_ref[d * cap : (d + 1) * cap] = block[:, width:]


def stacked_rows(blocks, width):
    count, cap = len(blocks), blocks[0].shape[0]
    return pl.pallas_call(
        functools.partial(stack_rows_kernel, width),
        out_shape=[
            jax.ShapeDtypeStruct((count * cap, width), jnp.bfloat16),
            jax.ShapeDtypeStruct((count * cap, LANES), jnp.bfloat16),
        ],
        in_specs=[VMEM] * count,
        out_specs=[VMEM] * 2,
        cost_estimate=cost(count * cap * width, 4 * count * cap * width),
        name="stack_rows",
    )(*blocks)


def stack_columns_kernel(*refs):
    experts = refs[0].shape[0]
    blocks, outs = refs[:-experts], refs[-experts:]
    part = blocks[0].shape[-1]
    for d, block in enumerate(blocks):
        for x, out in enumerate(outs):
            out[:, d * part : (d + 1) * part] = block[x]


def stacked_columns(blocks):
    count = len(blocks)
    experts, units, part = blocks[0].shape
    size = count * experts * units * part
    return pl.pallas_call(
        stack_columns_kernel,
        out_shape=[jax.ShapeDtypeStruct((units, count * part), jnp.bfloat16)] * experts,
        in_specs=[VMEM] * count,
        out_specs=[VMEM] * experts,
        cost_estimate=cost(size, 4 * size),
        name="stack_columns",
    )(*blocks)


def gathered(first, second, axis):
    count = lax.axis_size(axis)
    firsts, seconds = [first], [second]
    for e in range(1, count):
        low, high = e & -e, 1 << (e.bit_length() - 1)
        firsts.append(swap(firsts[e ^ low], axis, low))
        seconds.append(swap(seconds[e ^ high], axis, high))
    return firsts, seconds


def pre_kernel(matrix_ref, *refs):
    count = len(refs) // 2
    matrix = matrix_ref[...]
    for rows_ref, out_ref in zip(refs[:count], refs[count:]):
        out_ref[...] = nt_dot(rows_ref[...], matrix)


def gate_pre(rows, matrix):
    units, width = matrix.shape
    count = rows[0].shape[0]
    return pl.pallas_call(
        pre_kernel,
        out_shape=[jax.ShapeDtypeStruct((count, units), jnp.float32)] * len(rows),
        in_specs=[VMEM] * (1 + len(rows)),
        out_specs=[VMEM] * len(rows),
        cost_estimate=cost(2 * len(rows) * count * units * width, 2 * len(rows) * count * width),
        name="gate",
    )(matrix, *rows)


def active_kernel(count, parts, me_ref, *refs):
    pieces, refs = refs[:parts], refs[parts:]
    rows, gates, outs = refs[:count], refs[count : 2 * count], refs[2 * count : -1]
    matrix_ref = refs[-1]
    experts, units, part = pieces[0].shape
    for d, piece in enumerate(pieces):
        start = pl.multiple_of((me_ref[0] ^ d) * part, part)
        for x in range(experts):
            matrix_ref[x * units : (x + 1) * units, pl.ds(start, part)] = piece[x]
    matrix = matrix_ref[...]
    half = rows[0].shape[0]
    for e in range(count // 2):
        for h in range(2):
            up = nt_dot(rows[2 * e + h][...], matrix)
            gate = gates[2 * e + h][...]
            silu = gate / (1.0 + jnp.exp(-gate))
            outs[e][h * half : (h + 1) * half, :] = (silu * up).astype(jnp.bfloat16)


def active_units(me, rows, gates, pieces):
    if pieces[0].shape[-1] % LANES:
        pieces, me = [joined(me, pieces)[0]], jnp.zeros_like(me)
    experts, units, part = pieces[0].shape
    units, width = experts * units, part * len(pieces)
    half = rows[0].shape[0]
    count = len(rows)
    return pl.pallas_call(
        functools.partial(active_kernel, count, len(pieces)),
        out_shape=[jax.ShapeDtypeStruct((2 * half, units), jnp.bfloat16)] * (count // 2),
        in_specs=[pl.BlockSpec(memory_space=pltpu.SMEM)] + [VMEM] * (len(pieces) + 2 * count),
        out_specs=[VMEM] * (count // 2),
        scratch_shapes=[pltpu.VMEM((units, width), jnp.bfloat16)],
        cost_estimate=cost(2 * count * half * units * width, 2 * count * half * width),
        name="active",
    )(me, *pieces, *rows, *gates)


def mix_kernel(members, experts, near_ref, far_ref, *refs):
    hiddens, downs = refs[:members], refs[members : members * (1 + experts)]
    outs = refs[members * (1 + experts) :]
    cap = outs[0].shape[0]
    units = downs[0].shape[0]
    total = None
    for x in range(experts):
        hidden = jnp.concatenate([h[:, x * units : (x + 1) * units] for h in hiddens], axis=1)
        down = jnp.concatenate([d[...] for d in downs[x * members : (x + 1) * members]], axis=0)
        term = jnp.dot(hidden, down, preferred_element_type=jnp.float32)
        weight = jnp.concatenate([near_ref[:, x : x + 1], far_ref[:, x : x + 1]], axis=0)
        term = term * weight.astype(jnp.float32)
        total = term if total is None else total + term
    total = total.astype(jnp.bfloat16)
    for d, out in enumerate(outs):
        out[...] = total[d * cap : (d + 1) * cap]


def mixed_rows(weights, hiddens, downs, groups):
    members, experts = len(hiddens), len(downs)
    slots = hiddens[0].shape[0]
    units, width = downs[0][0].shape
    cap = slots // groups
    return pl.pallas_call(
        functools.partial(mix_kernel, members, experts),
        out_shape=[jax.ShapeDtypeStruct((cap, width), jnp.bfloat16)] * groups,
        in_specs=[VMEM] * (2 + members + members * experts),
        out_specs=[VMEM] * groups,
        cost_estimate=cost(
            2 * slots * members * experts * units * width, 2 * members * experts * units * width
        ),
        name="mixing",
    )(*weights, *hiddens, *[d for group in downs for d in group])


def finish_kernel(chunks, part, me_ref, placing_ref, *refs):
    out_ref, rows_ref = refs[-2], refs[-1]
    blocks = refs[:-2]
    per = len(blocks) // chunks
    cap, step = blocks[0].shape
    for c in range(chunks):
        for d in range(per):
            for k in range(step // part):
                start = pl.multiple_of((me_ref[0] ^ d ^ (c * (step // part) + k)) * part, part)
                rows_ref[d * cap : (d + 1) * cap, pl.ds(start, part)] = blocks[c * per + d][
                    :, k * part : (k + 1) * part
                ]
    out_ref[...] = lax.dot_general(
        placing_ref[...], rows_ref[...], (((0,), (0,)), ((), ())), preferred_element_type=jnp.float32
    ).astype(jnp.bfloat16)


def ordered(me, d, chunks, part):
    rows = jnp.concatenate(chunks, axis=1)
    cap, width = rows.shape
    count = width // part
    order = me[0] ^ d ^ jnp.arange(count)
    return rows.reshape(cap, count, part)[:, order].reshape(cap, width)


def finished(me, placing, chunks, part):
    slots, tokens = placing.shape
    width = sum(chunk[0].shape[1] for chunk in chunks)
    if part % LANES:
        rows = [ordered(me, d, [chunk[d] for chunk in chunks], part) for d in range(len(chunks[0]))]
        return lax.dot_general(
            placing, jnp.concatenate(rows), (((0,), (0,)), ((), ())), preferred_element_type=jnp.float32
        ).astype(jnp.bfloat16)
    flat = [b for chunk in chunks for b in chunk]
    return pl.pallas_call(
        functools.partial(finish_kernel, len(chunks), part),
        out_shape=jax.ShapeDtypeStruct((tokens, width), jnp.bfloat16),
        in_specs=[pl.BlockSpec(memory_space=pltpu.SMEM)] + [VMEM] * (1 + len(flat)),
        out_specs=VMEM,
        scratch_shapes=[pltpu.VMEM((slots, width), jnp.bfloat16)],
        cost_estimate=cost(2 * slots * tokens * width, 2 * slots * width),
        name="finish",
    )(me, placing, *flat)


def exchanged(blocks):
    got = {d: swap(blocks[d], "tp", d) for d in far_first(len(blocks))}
    return [blocks[0]] + [got[d] for d in range(1, len(blocks))]


def served(prompt, norm_gain, gate_master, up_master, down_master, group_pick, route_weight):
    groups, members = lax.axis_size("tp"), lax.axis_size("fs")
    width = prompt.shape[1]
    experts, units, part = gate_master.shape[1:]
    half = groups // 2
    me = lax.axis_index("tp").astype(jnp.int32).reshape(1)

    placing, send = route(me, prompt, group_pick, route_weight)
    rows = exchanged(send)
    gate_send = rounded(me, norm_gain, gate_master, True, placing)
    gate_parts = exchanged(gate_send)
    up_send = rounded(me, norm_gain, up_master, True, gate_send[0])
    up_parts = exchanged(up_send)
    down_send = rounded(me, norm_gain, down_master, False, up_send[0])
    down_parts = exchanged(down_send)

    near, near_weights = stacked_rows(rows[:half], width)
    far, far_weights = stacked_rows(rows[half:], width)
    weights = (near_weights, far_weights)
    firsts, seconds = gathered(near, far, "fs")
    all_rows = [r for pair in zip(firsts, seconds) for r in pair]
    near_down = gathered(*stacked_columns(down_parts[:half]), "fs")
    far_down = gathered(*stacked_columns(down_parts[half:]), "fs")

    gate_serve = joined(me, gate_parts)
    gates = gate_pre(all_rows, gate_serve.reshape(experts * units, width))
    active = active_units(me, all_rows, gates, up_parts)
    hiddens = [active[0]] + [swap(active[e], "fs", e) for e in range(1, members)]
    near_mix = mixed_rows(weights, hiddens, near_down, groups)
    near_back = exchanged(near_mix)
    far_mix = mixed_rows(weights, hiddens, far_down, groups)
    far_back = exchanged(far_mix)
    mixed = finished(me, placing, [near_back, far_back], part)
    up_serve = joined(me, up_parts)
    down_serve = joined(me, down_parts)
    return (gate_serve, up_serve, down_serve, mixed)


def solution(mesh):
    placed = (
        P(("fs", "tp"), None),
        P("tp"),
        P(None, None, "fs", "tp"),
        P(None, None, "fs", "tp"),
        P(None, None, "fs", "tp"),
        P(("fs", "tp"), None),
        P(("fs", "tp"), None),
    )
    return jax.shard_map(
        served,
        mesh=mesh,
        in_specs=placed,
        out_specs=(
            P("tp", None, "fs", None),
            P("tp", None, "fs", None),
            P("tp", None, "fs", None),
            P(("fs", "tp"), None),
        ),
        check_vma=False,
    )
```

profile of v0, /device:TPU:0, one launch (start us, length us, event | category | flops | bytes accessed | tf_op | source)
XLA Modules:
  0.0 219.2 jit_solution(377373309733820820)
XLA Ops:
  3.3 2.8 %rounding.3 = (bf16[2,128,256]{2,1,0:T(8,128)(2,1)}, bf16[2,128,256]{2,1,0:T(8,128)(2,1)}, bf16[2,128,256]{2,1,0:T(8,128)(2,1)}, bf16[2,128,256]{2,1,0:T(8,128)(...) custom-call(s32[1]{0:T(128)} %bitcast.me_ref, ...), custom_call_target="tpu_custom_call" | custom-call | flops 2097152 | bytes 3145728 | tf_op jit(solution)/shard_map/rounding/pallas_call | solution.py:98
  9.2 2.8 %collective-permute-start.3 = (bf16[2,128,256]{2,1,0:T(8,128)(2,1)}, bf16[2,128,256]{2,1,0:T(8,128)(2,1)S(1)}, u32[]{:S(2)}, u32[]{:S(2)}) collective-permute-start(bf16[2,128,256]{2,1,0:T(8,128)(2,1)} %get-tuple-element.78), channel_id=1, source_target_pairs={{0,4},{1,5},{2,6},{3,7},{4,0},{5,1},{6,2},{7,3},{8,12},{9,13},{10,... | collective-permute-start | bytes 393224 | tf_op jit(solution)/shard_map/ppermute | solution.py:26
  12.0 3.6 %collective-permute-start.5 = (bf16[2,128,256]{2,1,0:T(8,128)(2,1)}, bf16[2,128,256]{2,1,0:T(8,128)(2,1)S(1)}, u32[]{:S(2)}, u32[]{:S(2)}) collective-permute-start(bf16[2,128,256]{2,1,0:T(8,128)(2,1)} %get-tuple-element.80), channel_id=1, source_target_pairs={{0,6},{1,7},{2,4},{3,5},{4,2},{5,3},{6,0},{7,1},{8,14},{9,15},{10,... | collective-permute-start | bytes 393224 | tf_op jit(solution)/shard_map/ppermute | solution.py:26
  15.6 2.7 %rounding.4 = (bf16[2,128,256]{2,1,0:T(8,128)(2,1)}, bf16[2,128,256]{2,1,0:T(8,128)(2,1)}, bf16[2,128,256]{2,1,0:T(8,128)(2,1)}, bf16[2,128,256]{2,1,0:T(8,128)(...) custom-call(s32[1]{0:T(128)} %bitcast.me_ref, ...), custom_call_target="tpu_custom_call" | custom-call | flops 2097152 | bytes 3145728 | tf_op jit(solution)/shard_map/rounding/pallas_call | solution.py:98
  21.8 6.9 %collective-permute-start.8 = (bf16[2,128,256]{2,1,0:T(8,128)(2,1)}, bf16[2,128,256]{2,1,0:T(8,128)(2,1)S(1)}, u32[]{:S(2)}, u32[]{:S(2)}) collective-permute-start(bf16[2,128,256]{2,1,0:T(8,128)(2,1)} %get-tuple-element.84), channel_id=1, source_target_pairs={{0,2},{1,3},{2,0},{3,1},{4,6},{5,7},{6,4},{7,5},{8,10},{9,11},{10,... | collective-permute-start | bytes 393224 | tf_op jit(solution)/shard_map/ppermute | solution.py:26
  30.3 4.4 %collective-permute-start.22 = (bf16[32,2176]{1,0:T(8,128)(2,1)S(1)}, bf16[32,2176]{1,0:T(8,128)(2,1)S(1)}, u32[]{:S(2)}, u32[]{:S(2)}) collective-permute-start(bf16[32,2176]{1,0:T(8,128)(2,1)S(1)} %copy-done.62), channel_id=1, source_target_pairs={{0,2},{1,3},{2,0},{3,1},{4,6},{5,7},{6,4},{7,5},{8,10},{9,11},{10,... | collective-permute-start | bytes 417800 | tf_op jit(solution)/shard_map/ppermute | solution.py:26
  39.4 2.8 %collective-permute-start.26 = (bf16[32,2176]{1,0:T(8,128)(2,1)S(1)}, bf16[32,2176]{1,0:T(8,128)(2,1)S(1)}, u32[]{:S(2)}, u32[]{:S(2)}) collective-permute-start(bf16[32,2176]{1,0:T(8,128)(2,1)S(1)} %copy-done.58), channel_id=1, source_target_pairs={{0,6},{1,7},{2,4},{3,5},{4,2},{5,3},{6,0},{7,1},{8,14},{9,15},{10,... | collective-permute-start | bytes 417800 | tf_op jit(solution)/shard_map/ppermute | solution.py:26
  43.8 2.8 %collective-permute-start.10 = (bf16[2,128,256]{2,1,0:T(8,128)(2,1)}, bf16[2,128,256]{2,1,0:T(8,128)(2,1)S(1)}, u32[]{:S(2)}, u32[]{:S(2)}) collective-permute-start(bf16[2,128,256]{2,1,0:T(8,128)(2,1)} %get-tuple-element.86), channel_id=1, source_target_pairs={{0,4},{1,5},{2,6},{3,7},{4,0},{5,1},{6,2},{7,3},{8,12},{9,13},{10,... | collective-permute-start | bytes 393224 | tf_op jit(solution)/shard_map/ppermute | solution.py:26
  46.6 11.7 %collective-permute-done.25.refs_1_ = bf16[32,2176]{1,0:T(8,128)(2,1)S(1)} collective-permute-done((bf16[32,2176]{1,0:T(8,128)(2,1)S(1)}, bf16[32,2176]{1,0:T(8,128)(2,1)S(1)}, u32[]{:S(2)}, u32[]{:S(2)}) %collective-permute-start.25) | collective-permute-done | bytes 139296 | tf_op jit(solution)/shard_map/ppermute | solution.py:26
  58.4 4.9 %collective-permute-start.12 = (bf16[2,128,256]{2,1,0:T(8,128)(2,1)}, bf16[2,128,256]{2,1,0:T(8,128)(2,1)S(1)}, u32[]{:S(2)}, u32[]{:S(2)}) collective-permute-start(bf16[2,128,256]{2,1,0:T(8,128)(2,1)} %get-tuple-element.88), channel_id=1, source_target_pairs={{0,6},{1,7},{2,4},{3,5},{4,2},{5,3},{6,0},{7,1},{8,14},{9,15},{10,... | collective-permute-start | bytes 393224 | tf_op jit(solution)/shard_map/ppermute | solution.py:26
  63.3 2.7 %rounding.5 = (bf16[2,128,256]{2,1,0:T(8,128)(2,1)}, bf16[2,128,256]{2,1,0:T(8,128)(2,1)}, bf16[2,128,256]{2,1,0:T(8,128)(2,1)}, bf16[2,128,256]{2,1,0:T(8,128)(...) custom-call(s32[1]{0:T(128)} %bitcast.me_ref, ...), custom_call_target="tpu_custom_call" | custom-call | flops 2097152 | bytes 3145728 | tf_op jit(solution)/shard_map/rounding/pallas_call | solution.py:98
  66.0 4.2 %collective-permute-start.14 = (bf16[2,128,256]{2,1,0:T(8,128)(2,1)}, bf16[2,128,256]{2,1,0:T(8,128)(2,1)S(1)}, u32[]{:S(2)}, u32[]{:S(2)}) collective-permute-start(bf16[2,128,256]{2,1,0:T(8,128)(2,1)} %get-tuple-element.91), channel_id=1, source_target_pairs={{0,1},{1,0},{2,3},{3,2},{4,5},{5,4},{6,7},{7,6},{8,9},{9,8},{10,11... | collective-permute-start | bytes 393224 | tf_op jit(solution)/shard_map/ppermute | solution.py:26
  78.4 3.9 %collective-permute-start.15 = (bf16[2,128,256]{2,1,0:T(8,128)(2,1)}, bf16[2,128,256]{2,1,0:T(8,128)(2,1)S(1)}, u32[]{:S(2)}, u32[]{:S(2)}) collective-permute-start(bf16[2,128,256]{2,1,0:T(8,128)(2,1)} %get-tuple-element.92), channel_id=1, source_target_pairs={{0,2},{1,3},{2,0},{3,1},{4,6},{5,7},{6,4},{7,5},{8,10},{9,11},{10,... | collective-permute-start | bytes 393224 | tf_op jit(solution)/shard_map/ppermute | solution.py:26
  86.7 3.1 %collective-permute-start.17 = (bf16[2,128,256]{2,1,0:T(8,128)(2,1)}, bf16[2,128,256]{2,1,0:T(8,128)(2,1)S(1)}, u32[]{:S(2)}, u32[]{:S(2)}) collective-permute-start(bf16[2,128,256]{2,1,0:T(8,128)(2,1)} %get-tuple-element.94), channel_id=1, source_target_pairs={{0,4},{1,5},{2,6},{3,7},{4,0},{5,1},{6,2},{7,3},{8,12},{9,13},{10,... | collective-permute-start | bytes 393224 | tf_op jit(solution)/shard_map/ppermute | solution.py:26
  94.5 7.1 %collective-permute-done.17.refs_4_.refs_0_ = bf16[2,128,256]{2,1,0:T(8,128)(2,1)S(1)} collective-permute-done((bf16[2,128,256]{2,1,0:T(8,128)(2,1)}, bf16[2,128,256]{2,1,0:T(8,128)(2,1)S(1)}, u32[]{:S(2)}, u32[]{:S(2)}) %collective-permute-start.17) | collective-permute-done | bytes 131104 | tf_op jit(solution)/shard_map/ppermute | solution.py:26
  103.6 3.6 %collective-permute-start.20 = (bf16[2,128,256]{2,1,0:T(8,128)(2,1)}, bf16[2,128,256]{2,1,0:T(8,128)(2,1)S(1)}, u32[]{:S(2)}, u32[]{:S(2)}) collective-permute-start(bf16[2,128,256]{2,1,0:T(8,128)(2,1)} %get-tuple-element.97), channel_id=1, source_target_pairs={{0,7},{1,6},{2,5},{3,4},{4,3},{5,2},{6,1},{7,0},{8,15},{9,14},{10,... | collective-permute-start | bytes 393224 | tf_op jit(solution)/shard_map/ppermute | solution.py:26
  116.0 25.1 %collective-permute-done.40.refs_9_ = bf16[128,1024]{1,0:T(8,128)(2,1)} collective-permute-done((bf16[128,1024]{1,0:T(8,128)(2,1)}, bf16[128,1024]{1,0:T(8,128)(2,1)}, u32[]{:S(2)}, u32[]{:S(2)}) %collective-permute-start.40) | collective-permute-done | bytes 262176 | tf_op jit(solution)/shard_map/ppermute | solution.py:26
  150.5 6.0 %gate.1 = (f32[128,256]{1,0:T(8,128)}, f32[128,256]{1,0:T(8,128)}, f32[128,256]{1,0:T(8,128)}, f32[128,256]{1,0:T(8,128)}, f32[128,256]{1,0:T(8,128)}, /*index=5...) custom-call(bf16[256,2048]{1,0:T(8,128)(2,1)} %bitcast.5, ...), custom_call_target="tpu_custom_call" | custom-call | flops 1073741824 | bytes 4194304 | tf_op jit(solution)/shard_map/gate/pallas_call | solution.py:208
  156.5 6.5 %active.1 = (bf16[256,256]{1,0:T(8,128)(2,1)}, bf16[256,256]{1,0:T(8,128)(2,1)}, bf16[256,256]{1,0:T(8,128)(2,1)}, bf16[256,256]{1,0:T(8,128)(2,1)}) custom-call(s32[1]{0:T(128)} %bitcast.me_ref, bf16[2,128,256]{2,1,0:T(8,128)(2,1)} %get-tuple-element.82.refs_0_.after_ref, bf16[2,128,256]{2,1,0:T(8,128)(2,1)} %copy-done.6, bf16[2,128,256]{2,1,0:T(8,128)(2,1)} %copy-done.7, ...), custom_call_target="tpu_custom_call" | custom-call | flops 1073741824 | bytes 4194304 | tf_op jit(solution)/shard_map/active/pallas_call | solution.py:244
  173.1 9.7 %collective-permute-done.36.refs_3_ = bf16[256,256]{1,0:T(8,128)(2,1)S(1)} collective-permute-done((bf16[256,256]{1,0:T(8,128)(2,1)}, bf16[256,256]{1,0:T(8,128)(2,1)S(1)}, u32[]{:S(2)}, u32[]{:S(2)}) %collective-permute-start.36) | collective-permute-done | bytes 131104 | tf_op jit(solution)/shard_map/ppermute | solution.py:26
  183.4 3.2 %mixing.2 = (bf16[32,1024]{1,0:T(8,128)(2,1)}, bf16[32,1024]{1,0:T(8,128)(2,1)}, bf16[32,1024]{1,0:T(8,128)(2,1)}, bf16[32,1024]{1,0:T(8,128)(2,1)}, bf16[32,102...) custom-call(bf16[128,128]{1,0:T(8,128)(2,1)} %get-tuple-element.102.near_ref, ...), custom_call_target="tpu_custom_call" | custom-call | flops 536870912 | bytes 2097152 | tf_op jit(solution)/shard_map/mixing/pallas_call | solution.py:278
  186.8 3.3 %collective-permute-start.44 = (bf16[32,1024]{1,0:T(8,128)(2,1)}, bf16[32,1024]{1,0:T(8,128)(2,1)S(1)}, u32[]{:S(2)}, u32[]{:S(2)}) collective-permute-start(bf16[32,1024]{1,0:T(8,128)(2,1)} %get-tuple-element.126), channel_id=1, source_target_pairs={{0,2},{1,3},{2,0},{3,1},{4,6},{5,7},{6,4},{7,5},{8,10},{9,11},{10,... | collective-permute-start | bytes 196616 | tf_op jit(solution)/shard_map/ppermute | solution.py:26
  193.5 3.2 %mixing.3 = (bf16[32,1024]{1,0:T(8,128)(2,1)}, bf16[32,1024]{1,0:T(8,128)(2,1)}, bf16[32,1024]{1,0:T(8,128)(2,1)}, bf16[32,1024]{1,0:T(8,128)(2,1)}, bf16[32,102...) custom-call(bf16[128,128]{1,0:T(8,128)(2,1)} %get-tuple-element.102.near_ref, ...), custom_call_target="tpu_custom_call" | custom-call | flops 536870912 | bytes 2097152 | tf_op jit(solution)/shard_map/mixing/pallas_call | solution.py:278
  202.9 3.7 %collective-permute-start.59 = (bf16[32,1024]{1,0:T(8,128)(2,1)}, bf16[32,1024]{1,0:T(8,128)(2,1)S(1)}, u32[]{:S(2)}, u32[]{:S(2)}) collective-permute-start(bf16[32,1024]{1,0:T(8,128)(2,1)} %get-tuple-element.138), channel_id=1, source_target_pairs={{0,4},{1,5},{2,6},{3,7},{4,0},{5,1},{6,2},{7,3},{8,12},{9,13},{10,... | collective-permute-start | bytes 196616 | tf_op jit(solution)/shard_map/ppermute | solution.py:26
  (254 shorter events, 87.3 us)
Async XLA Ops:
  12.0 18.1 %collective-permute-start.4 = (bf16[2,128,256]{2,1,0:T(8,128)(2,1)}, bf16[2,128,256]{2,1,0:T(8,128)(2,1)S(1)}, u32[]{:S(2)}, u32[]{:S(2)}) collective-permute-start(bf16[2,128,256]{2,1,0:T(8,128)(2,1)} %get-tuple-element.79), channel_id=1, source_target_pairs={{0,5},{1,4},{2,7},{3,6},{4,1},{5,0},{6,3},{7,2},{8,13},{9,12},{10,... | collective-permute-start | bytes 393224 | tf_op jit(solution)/shard_map/ppermute | solution.py:26
  12.0 18.3 %collective-permute-start.5 = (bf16[2,128,256]{2,1,0:T(8,128)(2,1)}, bf16[2,128,256]{2,1,0:T(8,128)(2,1)S(1)}, u32[]{:S(2)}, u32[]{:S(2)}) collective-permute-start(bf16[2,128,256]{2,1,0:T(8,128)(2,1)} %get-tuple-element.80), channel_id=1, source_target_pairs={{0,6},{1,7},{2,4},{3,5},{4,2},{5,3},{6,0},{7,1},{8,14},{9,15},{10,... | collective-permute-start | bytes 393224 | tf_op jit(solution)/shard_map/ppermute | solution.py:26
  38.8 19.6 %collective-permute-start.25 = (bf16[32,2176]{1,0:T(8,128)(2,1)S(1)}, bf16[32,2176]{1,0:T(8,128)(2,1)S(1)}, u32[]{:S(2)}, u32[]{:S(2)}) collective-permute-start(bf16[32,2176]{1,0:T(8,128)(2,1)S(1)} %copy-done.59), channel_id=1, source_target_pairs={{0,5},{1,4},{2,7},{3,6},{4,1},{5,0},{6,3},{7,2},{8,13},{9,12},{10,... | collective-permute-start | bytes 417800 | tf_op jit(solution)/shard_map/ppermute | solution.py:26
  39.4 19.0 %collective-permute-start.26 = (bf16[32,2176]{1,0:T(8,128)(2,1)S(1)}, bf16[32,2176]{1,0:T(8,128)(2,1)S(1)}, u32[]{:S(2)}, u32[]{:S(2)}) collective-permute-start(bf16[32,2176]{1,0:T(8,128)(2,1)S(1)} %copy-done.58), channel_id=1, source_target_pairs={{0,6},{1,7},{2,4},{3,5},{4,2},{5,3},{6,0},{7,1},{8,14},{9,15},{10,... | collective-permute-start | bytes 417800 | tf_op jit(solution)/shard_map/ppermute | solution.py:26
  42.2 23.8 %collective-permute-start.27 = (bf16[32,2176]{1,0:T(8,128)(2,1)S(1)}, bf16[32,2176]{1,0:T(8,128)(2,1)S(1)}, u32[]{:S(2)}, u32[]{:S(2)}) collective-permute-start(bf16[32,2176]{1,0:T(8,128)(2,1)S(1)} %copy-done.57), channel_id=1, source_target_pairs={{0,7},{1,6},{2,5},{3,4},{4,3},{5,2},{6,1},{7,0},{8,15},{9,14},{10,... | collective-permute-start | bytes 417800 | tf_op jit(solution)/shard_map/ppermute | solution.py:26
  42.7 31.5 %collective-permute-start.9 = (bf16[2,128,256]{2,1,0:T(8,128)(2,1)}, bf16[2,128,256]{2,1,0:T(8,128)(2,1)S(1)}, u32[]{:S(2)}, u32[]{:S(2)}) collective-permute-start(bf16[2,128,256]{2,1,0:T(8,128)(2,1)} %get-tuple-element.85), channel_id=1, source_target_pairs={{0,3},{1,2},{2,1},{3,0},{4,7},{5,6},{6,5},{7,4},{8,11},{9,10},{10,... | collective-permute-start | bytes 393224 | tf_op jit(solution)/shard_map/ppermute | solution.py:26
  43.8 32.0 %collective-permute-start.10 = (bf16[2,128,256]{2,1,0:T(8,128)(2,1)}, bf16[2,128,256]{2,1,0:T(8,128)(2,1)S(1)}, u32[]{:S(2)}, u32[]{:S(2)}) collective-permute-start(bf16[2,128,256]{2,1,0:T(8,128)(2,1)} %get-tuple-element.86), channel_id=1, source_target_pairs={{0,4},{1,5},{2,6},{3,7},{4,0},{5,1},{6,2},{7,3},{8,12},{9,13},{10,... | collective-permute-start | bytes 393224 | tf_op jit(solution)/shard_map/ppermute | solution.py:26
  58.4 20.0 %collective-permute-start.11 = (bf16[2,128,256]{2,1,0:T(8,128)(2,1)}, bf16[2,128,256]{2,1,0:T(8,128)(2,1)S(1)}, u32[]{:S(2)}, u32[]{:S(2)}) collective-permute-start(bf16[2,128,256]{2,1,0:T(8,128)(2,1)} %get-tuple-element.87), channel_id=1, source_target_pairs={{0,5},{1,4},{2,7},{3,6},{4,1},{5,0},{6,3},{7,2},{8,13},{9,12},{10,... | collective-permute-start | bytes 393224 | tf_op jit(solution)/shard_map/ppermute | solution.py:26
  58.4 23.9 %collective-permute-start.12 = (bf16[2,128,256]{2,1,0:T(8,128)(2,1)}, bf16[2,128,256]{2,1,0:T(8,128)(2,1)S(1)}, u32[]{:S(2)}, u32[]{:S(2)}) collective-permute-start(bf16[2,128,256]{2,1,0:T(8,128)(2,1)} %get-tuple-element.88), channel_id=1, source_target_pairs={{0,6},{1,7},{2,4},{3,5},{4,2},{5,3},{6,0},{7,1},{8,14},{9,15},{10,... | collective-permute-start | bytes 393224 | tf_op jit(solution)/shard_map/ppermute | solution.py:26
  74.2 38.6 %collective-permute-start.30 = (bf16[128,2048]{1,0:T(8,128)(2,1)}, bf16[128,2048]{1,0:T(8,128)(2,1)S(1)}, u32[]{:S(2)}, u32[]{:S(2)}) collective-permute-start(bf16[128,2048]{1,0:T(8,128)(2,1)} %get-tuple-element.108.refs_0_.refs_8_), channel_id=1, source_target_pairs={{0,16},{8,24},{16,0},{24,8},{1,17},{9,25},{17,1},{25,9},{2,18},{10... | collective-permute-start | bytes 1572872 | tf_op jit(solution)/shard_map/ppermute | solution.py:26
  76.5 36.8 %collective-permute-start.29 = (bf16[128,2048]{1,0:T(8,128)(2,1)}, bf16[128,2048]{1,0:T(8,128)(2,1)S(1)}, u32[]{:S(2)}, u32[]{:S(2)}) collective-permute-start(bf16[128,2048]{1,0:T(8,128)(2,1)} %get-tuple-element.109.refs_1_.refs_9_), channel_id=1, source_target_pairs={{0,8},{8,0},{16,24},{24,16},{1,9},{9,1},{17,25},{25,17},{2,10},{10... | collective-permute-start | bytes 1572872 | tf_op jit(solution)/shard_map/ppermute | solution.py:26
  110.1 35.8 %collective-permute-start.28 = (bf16[128,2048]{1,0:T(8,128)(2,1)}, bf16[128,2048]{1,0:T(8,128)(2,1)S(1)}, u32[]{:S(2)}, u32[]{:S(2)}) collective-permute-start(bf16[128,2048]{1,0:T(8,128)(2,1)} %get-tuple-element.108.refs_0_.refs_8_), channel_id=1, source_target_pairs={{0,8},{8,0},{16,24},{24,16},{1,9},{9,1},{17,25},{25,17},{2,10},{10... | collective-permute-start | bytes 1572872 | tf_op jit(solution)/shard_map/ppermute | solution.py:26
  110.8 36.7 %collective-permute-start.31 = (bf16[128,2048]{1,0:T(8,128)(2,1)}, bf16[128,2048]{1,0:T(8,128)(2,1)S(1)}, u32[]{:S(2)}, u32[]{:S(2)}) collective-permute-start(bf16[128,2048]{1,0:T(8,128)(2,1)} %get-tuple-element.109.refs_1_.refs_9_), channel_id=1, source_target_pairs={{0,16},{8,24},{16,0},{24,8},{1,17},{9,25},{17,1},{25,9},{2,18},{10... | collective-permute-start | bytes 1572872 | tf_op jit(solution)/shard_map/ppermute | solution.py:26
  112.7 35.7 %collective-permute-start.32 = (bf16[128,2048]{1,0:T(8,128)(2,1)S(1)}, bf16[128,2048]{1,0:T(8,128)(2,1)S(1)}, u32[]{:S(2)}, u32[]{:S(2)}) collective-permute-start(bf16[128,2048]{1,0:T(8,128)(2,1)S(1)} %collective-permute-done.30.refs_4_.refs_12_), channel_id=1, source_target_pairs={{0,8},{8,0},{16,24},{24,16},{1,9},{9,1},{17,25},{25,17},{2,10},{10... | collective-permute-start | bytes 1572872 | tf_op jit(solution)/shard_map/ppermute | solution.py:26
  113.3 36.2 %collective-permute-start.33 = (bf16[128,2048]{1,0:T(8,128)(2,1)S(1)}, bf16[128,2048]{1,0:T(8,128)(2,1)S(1)}, u32[]{:S(2)}, u32[]{:S(2)}) collective-permute-start(bf16[128,2048]{1,0:T(8,128)(2,1)S(1)} %collective-permute-done.29.refs_3_.refs_11_), channel_id=1, source_target_pairs={{0,16},{8,24},{16,0},{24,8},{1,17},{9,25},{17,1},{25,9},{2,18},{10... | collective-permute-start | bytes 1572872 | tf_op jit(solution)/shard_map/ppermute | solution.py:26
  115.3 25.8 %collective-permute-start.40 = (bf16[128,1024]{1,0:T(8,128)(2,1)}, bf16[128,1024]{1,0:T(8,128)(2,1)}, u32[]{:S(2)}, u32[]{:S(2)}) collective-permute-start(bf16[128,1024]{1,0:T(8,128)(2,1)} %get-tuple-element.123.refs_8_), channel_id=1, source_target_pairs={{0,8},{8,0},{16,24},{24,16},{1,9},{9,1},{17,25},{25,17},{2,10},{10... | collective-permute-start | bytes 786440 | tf_op jit(solution)/shard_map/ppermute | solution.py:26
  141.1 21.9 %collective-permute-start.41 = (bf16[128,1024]{1,0:T(8,128)(2,1)}, bf16[128,1024]{1,0:T(8,128)(2,1)}, u32[]{:S(2)}, u32[]{:S(2)}) collective-permute-start(bf16[128,1024]{1,0:T(8,128)(2,1)} %get-tuple-element.123.refs_8_), channel_id=1, source_target_pairs={{0,16},{8,24},{16,0},{24,8},{1,17},{9,25},{17,1},{25,9},{2,18},{10... | collective-permute-start | bytes 786440 | tf_op jit(solution)/shard_map/ppermute | solution.py:26
  146.0 19.1 %collective-permute-start.51 = (bf16[128,1024]{1,0:T(8,128)(2,1)}, bf16[128,1024]{1,0:T(8,128)(2,1)}, u32[]{:S(2)}, u32[]{:S(2)}) collective-permute-start(bf16[128,1024]{1,0:T(8,128)(2,1)} %get-tuple-element.132.refs_4_), channel_id=1, source_target_pairs={{0,16},{8,24},{16,0},{24,8},{1,17},{9,25},{17,1},{25,9},{2,18},{10... | collective-permute-start | bytes 786440 | tf_op jit(solution)/shard_map/ppermute | solution.py:26
  147.5 18.3 %collective-permute-start.53 = (bf16[128,1024]{1,0:T(8,128)(2,1)}, bf16[128,1024]{1,0:T(8,128)(2,1)}, u32[]{:S(2)}, u32[]{:S(2)}) collective-permute-start(bf16[128,1024]{1,0:T(8,128)(2,1)} %get-tuple-element.133.refs_8_), channel_id=1, source_target_pairs={{0,8},{8,0},{16,24},{24,16},{1,9},{9,1},{17,25},{25,17},{2,10},{10... | collective-permute-start | bytes 786440 | tf_op jit(solution)/shard_map/ppermute | solution.py:26
  148.5 17.7 %collective-permute-start.39 = (bf16[128,1024]{1,0:T(8,128)(2,1)}, bf16[128,1024]{1,0:T(8,128)(2,1)}, u32[]{:S(2)}, u32[]{:S(2)}) collective-permute-start(bf16[128,1024]{1,0:T(8,128)(2,1)} %collective-permute-done.38.refs_6_), channel_id=1, source_target_pairs={{0,8},{8,0},{16,24},{24,16},{1,9},{9,1},{17,25},{25,17},{2,10},{10... | collective-permute-start | bytes 786440 | tf_op jit(solution)/shard_map/ppermute | solution.py:26
  165.8 20.9 %collective-permute-start.50 = (bf16[128,1024]{1,0:T(8,128)(2,1)S(1)}, bf16[128,1024]{1,0:T(8,128)(2,1)S(1)}, u32[]{:S(2)}, u32[]{:S(2)}) collective-permute-start(bf16[128,1024]{1,0:T(8,128)(2,1)S(1)} %copy-done.24), channel_id=1, source_target_pairs={{0,8},{8,0},{16,24},{24,16},{1,9},{9,1},{17,25},{25,17},{2,10},{10... | collective-permute-start | bytes 786440 | tf_op jit(solution)/shard_map/ppermute | solution.py:26
  166.2 23.9 %collective-permute-start.54 = (bf16[128,1024]{1,0:T(8,128)(2,1)S(1)}, bf16[128,1024]{1,0:T(8,128)(2,1)S(1)}, u32[]{:S(2)}, u32[]{:S(2)}) collective-permute-start(bf16[128,1024]{1,0:T(8,128)(2,1)S(1)} %copy-done.25), channel_id=1, source_target_pairs={{0,16},{8,24},{16,0},{24,8},{1,17},{9,25},{17,1},{25,9},{2,18},{10... | collective-permute-start | bytes 786440 | tf_op jit(solution)/shard_map/ppermute | solution.py:26
  167.2 23.0 %collective-permute-start.52 = (bf16[128,1024]{1,0:T(8,128)(2,1)}, bf16[128,1024]{1,0:T(8,128)(2,1)S(1)}, u32[]{:S(2)}, u32[]{:S(2)}) collective-permute-start(bf16[128,1024]{1,0:T(8,128)(2,1)} %collective-permute-done.51.refs_6_), channel_id=1, source_target_pairs={{0,8},{8,0},{16,24},{24,16},{1,9},{9,1},{17,25},{25,17},{2,10},{10... | collective-permute-start | bytes 786440 | tf_op jit(solution)/shard_map/ppermute | solution.py:26
  169.7 23.1 %collective-permute-start.55 = (bf16[128,1024]{1,0:T(8,128)(2,1)}, bf16[128,1024]{1,0:T(8,128)(2,1)S(1)}, u32[]{:S(2)}, u32[]{:S(2)}) collective-permute-start(bf16[128,1024]{1,0:T(8,128)(2,1)} %collective-permute-done.53.refs_9_), channel_id=1, source_target_pairs={{0,16},{8,24},{16,0},{24,8},{1,17},{9,25},{17,1},{25,9},{2,18},{10... | collective-permute-start | bytes 786440 | tf_op jit(solution)/shard_map/ppermute | solution.py:26
  (107 other events, 1583.6 us)
where the time goes:
time: 220 us; the launch traced here: 219 us
  starting transfers between devices  99.9 us (45%)
  waiting for transfers between devices  68.1 us (31%)
  Pallas kernels  46.9 us (21%)
  local copies, waits for them, and re-layouts  3.08 us (1%)
    ppermute x63, starting transfers between devices, swap(): return lax.ppermute(value, axis, [(i, i ^ distance) for i in range(count)])  99.9 us
    ppermute x63, waiting for transfers between devices, swap(): return lax.ppermute(value, axis, [(i, i ^ distance) for i in range(count)])  68.1 us
    pallas_call x3, Pallas kernels, rounded(): pl.pallas_call(functools.partial(round_kernel, scaled), out_shape=[block]...  8.16 us
    pallas_call x3, Pallas kernels, joined(): pl.pallas_call(kernel, out_shape=jax.ShapeDtypeStruct((1, experts, units,...  6.92 us
    pallas_call x1, Pallas kernels, active_units(): pl.pallas_call(functools.partial(active_kernel, count, len(pieces)), out_...  6.53 us
    pallas_call x2, Pallas kernels, mixed_rows(): pl.pallas_call(functools.partial(mix_kernel, members, experts), out_shape...  6.5 us
    pallas_call x1, Pallas kernels, gate_pre(): pl.pallas_call(pre_kernel, out_shape=[jax.ShapeDtypeStruct((count, units)...  5.96 us
  transfers between devices with their start and end apart: 63, of which 18 were waited for; matrix products, arithmetic and copies ran while one was open for 0% of the time, Pallas kernels for 18%

commit v1 on v0

v1 whole, which is shorter than its diff:
```python
import functools

import jax
import jax.numpy as jnp
from jax import lax
from jax.experimental import pallas as pl
from jax.experimental.pallas import tpu as pltpu
from jax.sharding import PartitionSpec as P


EPS = 1e-06
LANES = 128
BLOCKS = 2
VMEM = pl.BlockSpec(memory_space=pltpu.VMEM)


def nt_dot(left, right):
    return lax.dot_general(left, right, (((1,), (1,)), ((), ())), preferred_element_type=jnp.float32)


def cost(flops, moved):
    return pl.CostEstimate(flops=int(flops), bytes_accessed=int(moved), transcendentals=0)


def swap(value, axis, distance):
    count = lax.axis_size(axis)
    return lax.ppermute(value, axis, [(i, i ^ distance) for i in range(count)])


def route_kernel(cap, me_ref, prompt_ref, pick_ref, weight_ref, *out_refs):
    placing_ref, blocks = out_refs[0], out_refs[1:]
    slots, tokens = placing_ref.shape
    width = prompt_ref.shape[1]
    values = prompt_ref[...].astype(jnp.float32)
    scale = lax.rsqrt(jnp.mean(values * values, axis=1, keepdims=True) + EPS)
    normed = (values * scale).astype(jnp.bfloat16)
    distance = pick_ref[...] ^ me_ref[0]
    count = max(8, len(blocks))
    member = (lax.broadcasted_iota(jnp.int32, (count, tokens), 0) == distance).astype(jnp.float32)
    before = lax.broadcasted_iota(jnp.int32, (tokens, tokens), 0) < lax.broadcasted_iota(
        jnp.int32, (tokens, tokens), 1
    )
    earlier = jnp.dot(
        member.astype(jnp.bfloat16), before.astype(jnp.float32).astype(jnp.bfloat16),
        preferred_element_type=jnp.float32,
    )
    rank = jnp.sum(earlier * member, axis=0, keepdims=True).astype(jnp.int32)
    target = distance * cap + rank
    placing = (lax.broadcasted_iota(jnp.int32, (slots, tokens), 0) == target).astype(jnp.float32)
    placing = placing.astype(jnp.bfloat16)
    placing_ref[...] = placing
    weights = weight_ref[...].astype(jnp.float32)
    experts = weights.shape[0]
    row = lax.broadcasted_iota(jnp.int32, (LANES, tokens), 0)
    spread = jnp.zeros((LANES, tokens), jnp.float32)
    for x in range(experts):
        spread = jnp.where(row == x, weights[x : x + 1, :], spread)
    placed_weights = nt_dot(placing, spread.astype(jnp.bfloat16)).astype(jnp.bfloat16)
    rows = jnp.dot(placing, normed, preferred_element_type=jnp.float32).astype(jnp.bfloat16)
    for d, block in enumerate(blocks):
        block[:, :width] = rows[d * cap : (d + 1) * cap]
        block[:, width:] = placed_weights[d * cap : (d + 1) * cap]


def route(me, prompt, group_pick, route_weight):
    tokens, width = prompt.shape
    groups = lax.axis_size("tp")
    cap = 2 * tokens // groups
    block = jax.ShapeDtypeStruct((cap, width + LANES), jnp.bfloat16)
    outs = pl.pallas_call(
        functools.partial(route_kernel, cap),
        out_shape=[jax.ShapeDtypeStruct((groups * cap, tokens), jnp.bfloat16)] + [block] * groups,
        in_specs=[pl.BlockSpec(memory_space=pltpu.SMEM)] + [VMEM] * 3,
        out_specs=[VMEM] * (groups + 1),
        cost_estimate=cost(2 * groups * cap * tokens * width, 2 * tokens * width * 6),
        name="route",
    )(me, prompt, group_pick.reshape(1, tokens), route_weight.T)
    return outs[0], outs[1:]


def round_kernel(half, me_ref, gain_ref, gate_ref, up_ref, down_ref, *blocks):
    gain = gain_ref[...].reshape(1, 1, -1)
    near, far = blocks[:half], blocks[half:]
    for d in range(half + len(far) // 2):
        group = me_ref[0] ^ d
        pair, down = (near[d], near[d].at[2]) if d < half else (far[2 * (d - half)], far[2 * (d - half) + 1])
        pair[0] = (gate_ref[group] * gain).astype(jnp.bfloat16)
        pair[1] = (up_ref[group] * gain).astype(jnp.bfloat16)
        down[...] = down_ref[group].astype(jnp.bfloat16)


def rounded(me, gain, gate, up, down, after):
    groups, experts, units, part = gate.shape
    half = groups // 2
    shape = lambda *lead: jax.ShapeDtypeStruct((*lead, experts, units, part), jnp.bfloat16)
    size = 3 * groups * experts * units * part

    def kernel(me_ref, after_ref, *refs):
        round_kernel(half, me_ref, *refs)

    outs = pl.pallas_call(
        kernel,
        out_shape=[shape(3)] * half + [shape(2), shape()] * (groups - half),
        in_specs=[pl.BlockSpec(memory_space=pltpu.SMEM), pl.BlockSpec(memory_space=pl.ANY)] + [VMEM] * 4,
        out_specs=[VMEM] * (2 * groups - half),
        cost_estimate=cost(4 * size, 6 * size),
        name="rounding",
    )(me, after, gain.reshape(1, -1), gate, up, down)
    return outs[:half], outs[half::2], outs[half + 1 :: 2]


def parts_of(near, pairs, downs, which):
    if which == 2:
        return [ref[2] for ref in near] + list(downs)
    return [ref[which] for ref in near] + [ref[which] for ref in pairs]


def joined(me, near, pairs, downs):
    count = len(near) + len(pairs)
    _, experts, units, part = near[0].shape
    if part % LANES:
        order = me[0] ^ jnp.arange(count)
        outs = []
        for which in range(3):
            stack = jnp.stack(parts_of(near, pairs, downs, which))[order]
            outs.append(jnp.moveaxis(stack, 0, 2).reshape(1, experts, units, count * part))
        return outs
    sizes = (len(near), len(pairs), len(downs))

    def kernel(me_ref, *refs):
        ins, outs, sems = refs[: sum(sizes)], refs[sum(sizes) : -1], refs[-1]
        groups = ins[: sizes[0]], ins[sizes[0] : sizes[0] + sizes[1]], ins[sizes[0] + sizes[1] :]
        copies = []
        for which, out_ref in enumerate(outs):
            views = [[ref.at for ref in group] for group in groups[:2]]
            for d, piece in enumerate(parts_of(*views, groups[2], which)):
                start = pl.multiple_of((me_ref[0] ^ d) * part, part)
                copies.append(
                    pltpu.make_async_copy(
                        piece, out_ref.at[0, :, :, pl.ds(start, part)], sems.at[which, d]
                    )
                )
        for copy in copies:
            copy.start()
        for copy in copies:
            copy.wait()

    size = 3 * count * experts * units * part
    out = jax.ShapeDtypeStruct((1, experts, units, count * part), jnp.bfloat16)
    return pl.pallas_call(
        kernel,
        out_shape=[out] * 3,
        in_specs=[pl.BlockSpec(memory_space=pltpu.SMEM)] + [VMEM] * sum(sizes),
        out_specs=[pl.BlockSpec(memory_space=pl.ANY)] * 3,
        scratch_shapes=[pltpu.SemaphoreType.DMA((3, count))],
        cost_estimate=cost(4 * size, 4 * size),
        name="joining",
    )(me, *near, *pairs, *downs)


def stack_rows_kernel(width, *refs):
    blocks, rows_ref, weights_ref = refs[:-2], refs[-2], refs[-1]
    cap = blocks[0].shape[0]
    for d, block in enumerate(blocks):
        rows_ref[d * cap : (d + 1) * cap] = block[:, :width]
        weights_ref[d * cap : (d + 1) * cap] = block[:, width:]


def stacked_rows(blocks, width):
    count, cap = len(blocks), blocks[0].shape[0]
    return pl.pallas_call(
        functools.partial(stack_rows_kernel, width),
        out_shape=[
            jax.ShapeDtypeStruct((count * cap, width), jnp.bfloat16),
            jax.ShapeDtypeStruct((count * cap, LANES), jnp.bfloat16),
        ],
        in_specs=[VMEM] * count,
        out_specs=[VMEM] * 2,
        cost_estimate=cost(count * cap * width, 4 * count * cap * width),
        name="stack_rows",
    )(*blocks)


def stacked_columns(blocks, pieces):
    count = len(blocks)
    experts, units, part = blocks[0].shape[-3:]
    rows = experts * units // pieces

    def kernel(*refs):
        ins, outs = refs[:count], refs[count:]
        for d, block in enumerate(ins):
            piece = block.at[2] if len(block.shape) == 4 else block
            for x in range(experts):
                row = x * units % rows
                outs[x * units // rows][row : row + units, d * part : (d + 1) * part] = piece[x]

    size = count * experts * units * part
    return pl.pallas_call(
        kernel,
        out_shape=[jax.ShapeDtypeStruct((rows, count * part), jnp.bfloat16)] * pieces,
        in_specs=[VMEM] * count,
        out_specs=[VMEM] * pieces,
        cost_estimate=cost(size, 4 * size),
        name="stack_columns",
    )(*blocks)


def collected(value, axis):
    count = lax.axis_size(axis)
    return [value] + [swap(value, axis, e) for e in range(1, count)]


def gathered(first, second, axis):
    count = lax.axis_size(axis)
    firsts, seconds = [first], [second]
    for e in range(1, count):
        low, high = e & -e, 1 << (e.bit_length() - 1)
        firsts.append(swap(firsts[e ^ low], axis, low))
        seconds.append(swap(seconds[e ^ high], axis, high))
    return firsts, seconds


def active_kernel(first, parts, counts, me_ref, *refs):
    pieces, refs = refs[: counts[0]], refs[counts[0] :]
    rows, before, refs = refs[: counts[1]], refs[counts[1] : counts[1] + counts[2]], refs[sum(counts[1:3]) :]
    outs, (matrix_ref, rows_ref, sums_ref, sems) = refs[: counts[3]], refs[counts[3] :]
    _, experts, units, part = pieces[0].shape
    both = experts * units
    width = rows_ref.shape[2]
    place = lax.shift_right_logical(me_ref[0] ^ first, parts.bit_length() - 1)
    columns = pl.ds(pl.multiple_of(place * width, width), width)
    slots = rows[0].shape[0]
    spot = lambda b: rows_ref.at[b * slots // rows_ref.shape[1], pl.ds(b * slots % rows_ref.shape[1], slots)]
    copies = [
        pltpu.make_async_copy(ref.at[:, columns], spot(b), sems.at[0, b]) for b, ref in enumerate(rows)
    ]
    copies += [
        pltpu.make_async_copy(ref, sums_ref.at[b], sems.at[1, b]) for b, ref in enumerate(before)
    ]
    for copy in copies:
        copy.start()
    for d, piece in enumerate(pieces):
        start = pl.multiple_of(((me_ref[0] & (len(pieces) - 1)) ^ d) * part, part)
        for which in range(2):
            for x in range(experts):
                row = which * both + x * units
                matrix_ref[row : row + units, pl.ds(start, part)] = piece[which, x]
    group = rows_ref.shape[1] // slots
    for m in range(rows_ref.shape[0]):
        mine = range(m * group, (m + 1) * group)
        for b in mine:
            copies[b].wait()
        pre = nt_dot(rows_ref[m], matrix_ref[...])
        for b in mine:
            place = (b - m * group) * slots
            part_pre = pre[place : place + slots]
            if before:
                copies[len(rows) + b].wait()
                part_pre = part_pre + sums_ref[b]
            if len(outs) == len(rows):
                outs[b][...] = part_pre
            else:
                gate, up = part_pre[:, :both], part_pre[:, both:]
                silu = gate / (1.0 + jnp.exp(-gate))
                place = b % 2 * slots
                outs[b // 2][place : place + slots, :] = (silu * up).astype(jnp.bfloat16)


def active_units(me, rows, pieces, first, before, last):
    _, experts, units, part = pieces[0].shape
    parts = len(pieces)
    if part % LANES:
        order = (me[0] % parts) ^ jnp.arange(parts)
        stack = jnp.stack([block[:2] for block in pieces])[order]
        pieces = [jnp.moveaxis(stack, 0, 3).reshape(2, experts, units, parts * part)]
    slots, width = rows[0].shape[0], parts * part
    count, both = len(rows), experts * units
    if last:
        outs = [jax.ShapeDtypeStruct((2 * slots, both), jnp.bfloat16)] * (count // 2)
    else:
        outs = [jax.ShapeDtypeStruct((slots, 2 * both), jnp.float32)] * count
    counts = (len(pieces), count, len(before), len(outs))
    return pl.pallas_call(
        functools.partial(active_kernel, first, parts, counts),
        out_shape=outs,
        in_specs=[pl.BlockSpec(memory_space=pltpu.SMEM)]
        + [VMEM] * len(pieces)
        + [pl.BlockSpec(memory_space=pl.ANY)] * (count + len(before)),
        out_specs=[VMEM] * len(outs),
        scratch_shapes=[
            pltpu.VMEM((2 * both, width), jnp.bfloat16),
            pltpu.VMEM((BLOCKS, count * slots // BLOCKS, width), jnp.bfloat16),
            pltpu.VMEM((max(1, len(before)), slots, 2 * both), jnp.float32),
            pltpu.SemaphoreType.DMA((2, count)),
        ],
        cost_estimate=cost(4 * count * slots * both * width, 2 * count * slots * width),
        name="active",
    )(me, *pieces, *rows, *before)


def mix_kernel(members, experts, pieces, kept, near_ref, far_ref, *refs):
    hiddens, refs = refs[:members], refs[members:]
    number = members * sum(pieces)
    downs, kepts, outs = list(refs[:number]), refs[number : number + kept], refs[number + kept :]
    cap = outs[0].shape[0]
    for d, old in enumerate(kepts):
        outs[d][:, : old.shape[1]] = old[...]
    before = kepts[0].shape[1] if kept else 0
    begin = 0
    for piece in pieces:
        mine = [[downs.pop(0) for _ in range(piece)] for _ in range(members)]
        rows, width = mine[0][0].shape
        units = rows * piece // experts
        total = None
        for x in range(experts):
            row = x * units % rows
            hidden = jnp.concatenate([h[:, x * units : (x + 1) * units] for h in hiddens], axis=1)
            down = jnp.concatenate([d[x * units // rows][row : row + units] for d in mine], axis=0)
            term = jnp.dot(hidden, down, preferred_element_type=jnp.float32)
            weight = jnp.concatenate([near_ref[:, x : x + 1], far_ref[:, x : x + 1]], axis=0)
            term = term * weight.astype(jnp.float32)
            total = term if total is None else total + term
        total = total.astype(jnp.bfloat16)
        for d, out in enumerate(outs):
            place = begin + (before if d < kept else 0)
            out[:, place : place + width] = total[d * cap : (d + 1) * cap]
        begin += width


def mixed_rows(weights, hiddens, sets, kept, groups, experts):
    members = len(hiddens)
    slots = hiddens[0].shape[0]
    pieces = [len(downs[0]) for downs in sets]
    flat = [d for downs in sets for member in downs for d in member]
    width = sum(downs[0][0].shape[1] for downs in sets)
    cap = slots // groups
    before = kept[0].shape[1] if kept else 0
    out = lambda d: jax.ShapeDtypeStruct((cap, width + (before if d < len(kept) else 0)), jnp.bfloat16)
    size = members * hiddens[0].shape[1] * width
    return pl.pallas_call(
        functools.partial(mix_kernel, members, experts, pieces, len(kept)),
        out_shape=[out(d) for d in range(groups)],
        in_specs=[VMEM] * (2 + members + len(flat) + len(kept)),
        out_specs=[VMEM] * groups,
        cost_estimate=cost(2 * slots * size, 2 * size),
        name="mixing",
    )(*weights, *hiddens, *flat, *kept)


def finish_kernel(counts, part, me_ref, placing_ref, *refs):
    out_ref, rows_ref = refs[-2], refs[-1]
    blocks = list(refs[:-2])
    for d, count in enumerate(counts):
        base = 0
        for _ in range(count):
            block = blocks.pop(0)
            cap = block.shape[0]
            for k in range(block.shape[1] // part):
                start = pl.multiple_of((me_ref[0] ^ d ^ (base + k)) * part, part)
                rows_ref[d * cap : (d + 1) * cap, pl.ds(start, part)] = block[
                    :, k * part : (k + 1) * part
                ]
            base += block.shape[1] // part
    out_ref[...] = lax.dot_general(
        placing_ref[...], rows_ref[...], (((0,), (0,)), ((), ())), preferred_element_type=jnp.float32
    ).astype(jnp.bfloat16)


def ordered(me, d, chunks, part):
    rows = jnp.concatenate(chunks, axis=1)
    cap, width = rows.shape
    count = width // part
    order = me[0] ^ d ^ jnp.arange(count)
    return rows.reshape(cap, count, part)[:, order].reshape(cap, width)


def finished(me, placing, back, part):
    slots, tokens = placing.shape
    width = sum(block.shape[1] for block in back[0])
    if part % LANES:
        rows = [ordered(me, d, blocks, part) for d, blocks in enumerate(back)]
        return lax.dot_general(
            placing, jnp.concatenate(rows), (((0,), (0,)), ((), ())), preferred_element_type=jnp.float32
        ).astype(jnp.bfloat16)
    flat = [b for blocks in back for b in blocks]
    counts = [len(blocks) for blocks in back]
    return pl.pallas_call(
        functools.partial(finish_kernel, counts, part),
        out_shape=jax.ShapeDtypeStruct((tokens, width), jnp.bfloat16),
        in_specs=[pl.BlockSpec(memory_space=pltpu.SMEM)] + [VMEM] * (1 + len(flat)),
        out_specs=VMEM,
        scratch_shapes=[pltpu.VMEM((slots, width), jnp.bfloat16)],
        cost_estimate=cost(2 * slots * tokens * width, 2 * slots * width),
        name="finish",
    )(me, placing, *flat)


def sent(blocks, first):
    return [block if d == 0 else swap(block, "tp", d) for d, block in enumerate(blocks, start=first)]


def served(prompt, norm_gain, gate_master, up_master, down_master, group_pick, route_weight):
    groups, members = lax.axis_size("tp"), lax.axis_size("fs")
    width = prompt.shape[1]
    experts, _, part = gate_master.shape[1:]
    half = groups // 2
    me = lax.axis_index("tp").astype(jnp.int32).reshape(1)

    placing, send = route(me, prompt, group_pick, route_weight)
    rows = sent(send, 0)
    near, pairs, downs = rounded(me, norm_gain, gate_master, up_master, down_master, placing)
    near, pairs, downs = sent(near, 0), sent(pairs, half), sent(downs, half)

    near_rows, near_weights = stacked_rows(rows[:half], width)
    far_rows, far_weights = stacked_rows(rows[half:], width)
    weights = (near_weights, far_weights)
    firsts, seconds = gathered(near_rows, far_rows, "fs")
    all_rows = [r for pair in zip(firsts, seconds) for r in pair]
    cut = (groups - half) // 2
    sums = active_units(me, all_rows, near, 0, [], False)
    sums = active_units(me, all_rows, pairs[:cut], half, sums, False)
    active = active_units(me, all_rows, pairs[cut:], half + cut, sums, True)
    hiddens = [active[0]] + [swap(active[e], "fs", e) for e in range(1, members)]
    sides = gathered(*stacked_columns(near, 2), "fs")
    sets = [list(zip(*sides))]
    for blocks in (downs[:cut], downs[cut:]):
        whole = stacked_columns(blocks, 1)[0]
        sets.append([[one] for one in collected(whole, "fs")])
    early = mixed_rows(weights, hiddens, sets[:2], [], groups, experts)
    late = mixed_rows(weights, hiddens, sets[2:], early[:half], groups, experts)
    back = [[block] for block in sent(late[:half], 0)]
    back += zip(sent(early[half:], half), sent(late[half:], half))
    mixed = finished(me, placing, back, part)
    gate_serve, up_serve, down_serve = joined(me, near, pairs, downs)
    return (gate_serve, up_serve, down_serve, mixed)


def solution(mesh):
    placed = (
        P(("fs", "tp"), None),
        P("tp"),
        P(None, None, "fs", "tp"),
        P(None, None, "fs", "tp"),
        P(None, None, "fs", "tp"),
        P(("fs", "tp"), None),
        P(("fs", "tp"), None),
    )
    return jax.shard_map(
        served,
        mesh=mesh,
        in_specs=placed,
        out_specs=(
            P("tp", None, "fs", None),
            P("tp", None, "fs", None),
            P("tp", None, "fs", None),
            P(("fs", "tp"), None),
        ),
        check_vma=False,
    )
```

time: 220 us -> 226 us (1.027)
  waiting for transfers between devices: 68.1 us -> 82.6 us
  starting transfers between devices: 99.9 us -> 92.6 us
  Pallas kernels: 46.9 us -> 44.2 us
    ppermute x63 -> x50, waiting for transfers between devices: 68.1 us -> 82.6 us  [swap(): return lax.ppermute(value, axis, [(i, i ^ distance) for i in range(count)])]
    ppermute x63 -> x50, starting transfers between devices: 99.9 us -> 92.6 us  [swap(): return lax.ppermute(value, axis, [(i, i ^ distance) for i in range(count)])]
    pallas_call x13 -> x11, Pallas kernels: 40.4 us -> 37.6 us  [the longest x3 14.3 us: active_units(): pl.pallas_call(functools.partial(active_kernel, first, parts, counts), ou...]
    unnamed x136 -> x106, local copies, waits for them, and re-layouts: 3.08 us -> 4.53 us
  transfers between devices with their start and end apart: 63 -> 50, of which waited for: 18 -> 14; matrix products, arithmetic and copies ran while one was open for 0% -> 0% of each run, Pallas kernels for 18% -> 15%
where the time goes in v1:
time: 226 us; the launch traced here: 225 us
  starting transfers between devices  92.6 us (41%)
  waiting for transfers between devices  82.6 us (37%)
  Pallas kernels  44.2 us (20%)
  local copies, waits for them, and re-layouts  4.53 us (2%)
    ppermute x50, starting transfers between devices, swap(): return lax.ppermute(value, axis, [(i, i ^ distance) for i in range(count)])  92.6 us
    ppermute x50, waiting for transfers between devices, swap(): return lax.ppermute(value, axis, [(i, i ^ distance) for i in range(count)])  82.6 us
    pallas_call x3, Pallas kernels, active_units(): pl.pallas_call(functools.partial(active_kernel, first, parts, counts), ou...  14.3 us
    pallas_call x2, Pallas kernels, mixed_rows(): pl.pallas_call(functools.partial(mix_kernel, members, experts, pieces, le...  6.71 us
    pallas_call x3, Pallas kernels, stacked_columns(): pl.pallas_call(kernel, out_shape=[jax.ShapeDtypeStruct((rows, count * par...  5.57 us
    pallas_call x1, Pallas kernels, rounded(): pl.pallas_call(kernel, out_shape=[shape(3)] * half + [shape(2), shape()]...  4.9 us
    unnamed x106, local copies, waits for them, and re-layouts  4.53 us
  transfers between devices with their start and end apart: 50, of which 14 were waited for; matrix products, arithmetic and copies ran while one was open for 0% of the time, Pallas kernels for 15%

profile of v1, /device:TPU:0, one launch (start us, length us, event | category | flops | bytes accessed | tf_op | source)
XLA Modules:
  0.0 224.9 jit_solution(252858749349959540)
XLA Ops:
  0.6 2.6 %route.1 = (bf16[256,128]{1,0:T(8,128)(2,1)}, bf16[32,2176]{1,0:T(8,128)(2,1)}, bf16[32,2176]{1,0:T(8,128)(2,1)}, bf16[32,2176]{1,0:T(8,128)(2,1)}, bf16[32,2176...) custom-call(s32[1]{0:T(128)} %bitcast.me_ref, ...), custom_call_target="tpu_custom_call" | custom-call | flops 134217728 | bytes 3145728 | tf_op jit(solution)/shard_map/route/pallas_call | solution.py:70
  3.3 4.9 %rounding.1 = (bf16[3,2,128,256]{3,2,1,0:T(8,128)(2,1)}, bf16[3,2,128,256]{3,2,1,0:T(8,128)(2,1)}, bf16[3,2,128,256]{3,2,1,0:T(8,128)(2,1)}, bf16[3,2,128,256]{3...) custom-call(s32[1]{0:T(128)} %bitcast.me_ref, ...), custom_call_target="tpu_custom_call" | custom-call | flops 6291456 | bytes 9437184 | tf_op jit(solution)/shard_map/rounding/pallas_call | solution.py:101
  8.2 4.1 %collective-permute-start.7 = (bf16[2,128,256]{2,1,0:T(8,128)(2,1)}, bf16[2,128,256]{2,1,0:T(8,128)(2,1)S(1)}, u32[]{:S(2)}, u32[]{:S(2)}) collective-permute-start(bf16[2,128,256]{2,1,0:T(8,128)(2,1)} %get-tuple-element.79), channel_id=1, source_target_pairs={{0,4},{1,5},{2,6},{3,7},{4,0},{5,1},{6,2},{7,3},{8,12},{9,13},{10,... | collective-permute-start | bytes 393224 | tf_op jit(solution)/shard_map/ppermute | solution.py:27
  16.0 2.5 %collective-permute-start.9 = (bf16[2,128,256]{2,1,0:T(8,128)(2,1)}, bf16[2,128,256]{2,1,0:T(8,128)(2,1)S(1)}, u32[]{:S(2)}, u32[]{:S(2)}) collective-permute-start(bf16[2,128,256]{2,1,0:T(8,128)(2,1)} %get-tuple-element.81), channel_id=1, source_target_pairs={{0,6},{1,7},{2,4},{3,5},{4,2},{5,3},{6,0},{7,1},{8,14},{9,15},{10,... | collective-permute-start | bytes 393224 | tf_op jit(solution)/shard_map/ppermute | solution.py:27
  18.4 12.6 %collective-permute-done.7.refs_8_.refs_0_ = bf16[2,128,256]{2,1,0:T(8,128)(2,1)S(1)} collective-permute-done((bf16[2,128,256]{2,1,0:T(8,128)(2,1)}, bf16[2,128,256]{2,1,0:T(8,128)(2,1)S(1)}, u32[]{:S(2)}, u32[]{:S(2)}) %collective-permute-start.7) | collective-permute-done | bytes 131104 | tf_op jit(solution)/shard_map/ppermute | solution.py:27
  32.1 7.3 %collective-permute-start.16 = (bf16[32,2176]{1,0:T(8,128)(2,1)S(1)}, bf16[32,2176]{1,0:T(8,128)(2,1)S(1)}, u32[]{:S(2)}, u32[]{:S(2)}) collective-permute-start(bf16[32,2176]{1,0:T(8,128)(2,1)S(1)} %copy-done.50), channel_id=1, source_target_pairs={{0,6},{1,7},{2,4},{3,5},{4,2},{5,3},{6,0},{7,1},{8,14},{9,15},{10,... | collective-permute-start | bytes 417800 | tf_op jit(solution)/shard_map/ppermute | solution.py:27
  39.8 13.6 %collective-permute-start.3 = (bf16[2,2,128,256]{3,2,1,0:T(8,128)(2,1)}, bf16[2,2,128,256]{3,2,1,0:T(8,128)(2,1)S(1)}, u32[]{:S(2)}, u32[]{:S(2)}) collective-permute-start(bf16[2,2,128,256]{3,2,1,0:T(8,128)(2,1)} %get-tuple-element.75), channel_id=1, source_target_pairs={{0,4},{1,5},{2,6},{3,7},{4,0},{5,1},{6,2},{7,3},{8,12},{9,13},{10,... | collective-permute-start | bytes 786440 | tf_op jit(solution)/shard_map/ppermute | solution.py:27
  54.4 8.1 %collective-permute-start.13 = (bf16[32,2176]{1,0:T(8,128)(2,1)S(1)}, bf16[32,2176]{1,0:T(8,128)(2,1)S(1)}, u32[]{:S(2)}, u32[]{:S(2)}) collective-permute-start(bf16[32,2176]{1,0:T(8,128)(2,1)S(1)} %copy-done.46), channel_id=1, source_target_pairs={{0,3},{1,2},{2,1},{3,0},{4,7},{5,6},{6,5},{7,4},{8,11},{9,10},{10,... | collective-permute-start | bytes 417800 | tf_op jit(solution)/shard_map/ppermute | solution.py:27
  62.5 4.9 %collective-permute-start.4 = (bf16[2,2,128,256]{3,2,1,0:T(8,128)(2,1)}, bf16[2,2,128,256]{3,2,1,0:T(8,128)(2,1)S(1)}, u32[]{:S(2)}, u32[]{:S(2)}) collective-permute-start(bf16[2,2,128,256]{3,2,1,0:T(8,128)(2,1)} %get-tuple-element.76), channel_id=1, source_target_pairs={{0,5},{1,4},{2,7},{3,6},{4,1},{5,0},{6,3},{7,2},{8,13},{9,12},{10,... | collective-permute-start | bytes 786440 | tf_op jit(solution)/shard_map/ppermute | solution.py:27
  68.3 2.7 %collective-permute-done.13.refs_3_ = bf16[32,2176]{1,0:T(8,128)(2,1)S(1)} collective-permute-done((bf16[32,2176]{1,0:T(8,128)(2,1)S(1)}, bf16[32,2176]{1,0:T(8,128)(2,1)S(1)}, u32[]{:S(2)}, u32[]{:S(2)}) %collective-permute-start.13) | collective-permute-done | bytes 139296 | tf_op jit(solution)/shard_map/ppermute | solution.py:27
  71.5 11.5 %collective-permute-done.3.refs_4_.refs_0_ = bf16[2,2,128,256]{3,2,1,0:T(8,128)(2,1)S(1)} collective-permute-done((bf16[2,2,128,256]{3,2,1,0:T(8,128)(2,1)}, bf16[2,2,128,256]{3,2,1,0:T(8,128)(2,1)S(1)}, u32[]{:S(2)}, u32[]{:S(2)}) %collective-permute-start.3) | collective-permute-done | bytes 262176 | tf_op jit(solution)/shard_map/ppermute | solution.py:27
  91.8 2.9 %collective-permute-start.6 = (bf16[2,2,128,256]{3,2,1,0:T(8,128)(2,1)}, bf16[2,2,128,256]{3,2,1,0:T(8,128)(2,1)}, u32[]{:S(2)}, u32[]{:S(2)}) collective-permute-start(bf16[2,2,128,256]{3,2,1,0:T(8,128)(2,1)} %get-tuple-element.78), channel_id=1, source_target_pairs={{0,7},{1,6},{2,5},{3,4},{4,3},{5,2},{6,1},{7,0},{8,15},{9,14},{10,... | collective-permute-start | bytes 786440 | tf_op jit(solution)/shard_map/ppermute | solution.py:27
  97.0 11.9 %collective-permute-done.2.refs_3_ = bf16[3,2,128,256]{3,2,1,0:T(8,128)(2,1)S(1)} collective-permute-done((bf16[3,2,128,256]{3,2,1,0:T(8,128)(2,1)}, bf16[3,2,128,256]{3,2,1,0:T(8,128)(2,1)S(1)}, u32[]{:S(2)}, u32[]{:S(2)}) %collective-permute-start.2) | collective-permute-done | bytes 393248 | tf_op jit(solution)/shard_map/ppermute | solution.py:27
  114.6 3.8 %collective-permute-done.37.refs_14_ = bf16[256,512]{1,0:T(8,128)(2,1)} collective-permute-done((bf16[256,512]{1,0:T(8,128)(2,1)}, bf16[256,512]{1,0:T(8,128)(2,1)}, u32[]{:S(2)}, u32[]{:S(2)}) %collective-permute-start.37) | collective-permute-done | bytes 262176 | tf_op jit(solution)/shard_map/ppermute | solution.py:27
  125.4 21.9 %collective-permute-done.31.refs_7_ = bf16[128,1024]{1,0:T(8,128)(2,1)} collective-permute-done((bf16[128,1024]{1,0:T(8,128)(2,1)}, bf16[128,1024]{1,0:T(8,128)(2,1)}, u32[]{:S(2)}, u32[]{:S(2)}) %collective-permute-start.31) | collective-permute-done | bytes 262176 | tf_op jit(solution)/shard_map/ppermute | solution.py:27
  154.5 5.1 %active.3 = (f32[128,512]{1,0:T(8,128)}, f32[128,512]{1,0:T(8,128)}, f32[128,512]{1,0:T(8,128)}, f32[128,512]{1,0:T(8,128)}, f32[128,512]{1,0:T(8,128)}, /*index...) custom-call(s32[1]{0:T(128)} %bitcast.me_ref, bf16[3,2,128,256]{3,2,1,0:T(8,128)(2,1)} %get-tuple-element.71.refs_0_, ...), custom_call_target="tpu_custom_call" | custom-call | flops 1073741824 | bytes 2097152 | tf_op jit(solution)/shard_map/active/pallas_call | solution.py:283
  159.6 4.8 %active.4 = (f32[128,512]{1,0:T(8,128)}, f32[128,512]{1,0:T(8,128)}, f32[128,512]{1,0:T(8,128)}, f32[128,512]{1,0:T(8,128)}, f32[128,512]{1,0:T(8,128)}, /*index...) custom-call(s32[1]{0:T(128)} %bitcast.me_ref, bf16[2,2,128,256]{3,2,1,0:T(8,128)(2,1)} %copy-done.11, ...), custom_call_target="tpu_custom_call" | custom-call | flops 536870912 | bytes 1048576 | tf_op jit(solution)/shard_map/active/pallas_call | solution.py:283
  164.4 4.4 %active.5 = (bf16[256,256]{1,0:T(8,128)(2,1)}, bf16[256,256]{1,0:T(8,128)(2,1)}, bf16[256,256]{1,0:T(8,128)(2,1)}, bf16[256,256]{1,0:T(8,128)(2,1)}) custom-call(s32[1]{0:T(128)} %bitcast.me_ref, bf16[2,2,128,256]{3,2,1,0:T(8,128)(2,1)} %copy-done.13, bf16[2,2,128,256]{3,2,1,0:T(8,128)(2,1)} %collective-permute-done.6.refs_7_.refs_1_, ...), custom_call_target="tpu_custom_call" | custom-call | flops 536870912 | bytes 1048576 | tf_op jit(solution)/shard_map/active/pallas_call | solution.py:283
  177.6 9.9 %collective-permute-done.25.refs_2_ = bf16[256,256]{1,0:T(8,128)(2,1)S(1)} collective-permute-done((bf16[256,256]{1,0:T(8,128)(2,1)}, bf16[256,256]{1,0:T(8,128)(2,1)S(1)}, u32[]{:S(2)}, u32[]{:S(2)}) %collective-permute-start.25) | collective-permute-done | bytes 131104 | tf_op jit(solution)/shard_map/ppermute | solution.py:27
  188.2 3.9 %mixing.2 = (bf16[32,1536]{1,0:T(8,128)(2,1)}, bf16[32,1536]{1,0:T(8,128)(2,1)}, bf16[32,1536]{1,0:T(8,128)(2,1)}, bf16[32,1536]{1,0:T(8,128)(2,1)}, bf16[32,153...) custom-call(bf16[128,128]{1,0:T(8,128)(2,1)} %get-tuple-element.90.near_ref, ...), custom_call_target="tpu_custom_call" | custom-call | flops 805306368 | bytes 3145728 | tf_op jit(solution)/shard_map/mixing/pallas_call | solution.py:340
  195.1 2.8 %mixing.3 = (bf16[32,2048]{1,0:T(8,128)(2,1)}, bf16[32,2048]{1,0:T(8,128)(2,1)}, bf16[32,2048]{1,0:T(8,128)(2,1)}, bf16[32,2048]{1,0:T(8,128)(2,1)}, bf16[32,512...) custom-call(bf16[128,128]{1,0:T(8,128)(2,1)} %get-tuple-element.90.near_ref, ...), custom_call_target="tpu_custom_call" | custom-call | flops 268435456 | bytes 1048576 | tf_op jit(solution)/shard_map/mixing/pallas_call | solution.py:340
  201.2 4.2 %collective-permute-start.47 = (bf16[32,512]{1,0:T(8,128)(2,1)}, bf16[32,512]{1,0:T(8,128)(2,1)S(1)}, u32[]{:S(2)}, u32[]{:S(2)}) collective-permute-start(bf16[32,512]{1,0:T(8,128)(2,1)} %get-tuple-element.133), channel_id=1, source_target_pairs={{0,6},{1,7},{2,4},{3,5},{4,2},{5,3},{6,0},{7,1},{8,14},{9,15},{10,... | collective-permute-start | bytes 98312 | tf_op jit(solution)/shard_map/ppermute | solution.py:27
  210.7 3.9 %collective-permute-start.46 = (bf16[32,1536]{1,0:T(8,128)(2,1)}, bf16[32,1536]{1,0:T(8,128)(2,1)S(1)}, u32[]{:S(2)}, u32[]{:S(2)}) collective-permute-start(bf16[32,1536]{1,0:T(8,128)(2,1)} %get-tuple-element.132), channel_id=1, source_target_pairs={{0,6},{1,7},{2,4},{3,5},{4,2},{5,3},{6,0},{7,1},{8,14},{9,15},{10,... | collective-permute-start | bytes 294920 | tf_op jit(solution)/shard_map/ppermute | solution.py:27
  214.6 3.7 %joining.1 = (bf16[1,2,128,2048]{3,2,1,0:T(8,128)(2,1)}, bf16[1,2,128,2048]{3,2,1,0:T(8,128)(2,1)}, bf16[1,2,128,2048]{3,2,1,0:T(8,128)(2,1)}) custom-call(s32[1]{0:T(128)} %bitcast.me_ref, bf16[3,2,128,256]{3,2,1,0:T(8,128)(2,1)} %get-tuple-element.71.refs_0_, bf16[3,2,128,256]{3,2,1,0:T(8,128)(2,1)} %copy-done.8, bf16[3,2,128,256]{3,2,1,0:T(8,128)(2,1)} %copy-done.9, ...), custom_call_target="tpu_custom_call" | custom-call | flops 6291456 | bytes 6291456 | tf_op jit(solution)/shard_map/joining/pallas_call | solution.py:150
  (196 shorter events, 66.1 us)
Async XLA Ops:
  8.2 22.8 %collective-permute-start.7 = (bf16[2,128,256]{2,1,0:T(8,128)(2,1)}, bf16[2,128,256]{2,1,0:T(8,128)(2,1)S(1)}, u32[]{:S(2)}, u32[]{:S(2)}) collective-permute-start(bf16[2,128,256]{2,1,0:T(8,128)(2,1)} %get-tuple-element.79), channel_id=1, source_target_pairs={{0,4},{1,5},{2,6},{3,7},{4,0},{5,1},{6,2},{7,3},{8,12},{9,13},{10,... | collective-permute-start | bytes 393224 | tf_op jit(solution)/shard_map/ppermute | solution.py:27
  12.3 27.5 %collective-permute-start.14 = (bf16[32,2176]{1,0:T(8,128)(2,1)S(1)}, bf16[32,2176]{1,0:T(8,128)(2,1)S(1)}, u32[]{:S(2)}, u32[]{:S(2)}) collective-permute-start(bf16[32,2176]{1,0:T(8,128)(2,1)S(1)} %copy-done.52), channel_id=1, source_target_pairs={{0,4},{1,5},{2,6},{3,7},{4,0},{5,1},{6,2},{7,3},{8,12},{9,13},{10,... | collective-permute-start | bytes 417800 | tf_op jit(solution)/shard_map/ppermute | solution.py:27
  14.3 25.1 %collective-permute-start.10 = (bf16[2,128,256]{2,1,0:T(8,128)(2,1)}, bf16[2,128,256]{2,1,0:T(8,128)(2,1)S(1)}, u32[]{:S(2)}, u32[]{:S(2)}) collective-permute-start(bf16[2,128,256]{2,1,0:T(8,128)(2,1)} %get-tuple-element.82), channel_id=1, source_target_pairs={{0,7},{1,6},{2,5},{3,4},{4,3},{5,2},{6,1},{7,0},{8,15},{9,14},{10,... | collective-permute-start | bytes 393224 | tf_op jit(solution)/shard_map/ppermute | solution.py:27
  16.0 23.5 %collective-permute-start.9 = (bf16[2,128,256]{2,1,0:T(8,128)(2,1)}, bf16[2,128,256]{2,1,0:T(8,128)(2,1)S(1)}, u32[]{:S(2)}, u32[]{:S(2)}) collective-permute-start(bf16[2,128,256]{2,1,0:T(8,128)(2,1)} %get-tuple-element.81), channel_id=1, source_target_pairs={{0,6},{1,7},{2,4},{3,5},{4,2},{5,3},{6,0},{7,1},{8,14},{9,15},{10,... | collective-permute-start | bytes 393224 | tf_op jit(solution)/shard_map/ppermute | solution.py:27
  31.0 22.3 %collective-permute-start.15 = (bf16[32,2176]{1,0:T(8,128)(2,1)S(1)}, bf16[32,2176]{1,0:T(8,128)(2,1)S(1)}, u32[]{:S(2)}, u32[]{:S(2)}) collective-permute-start(bf16[32,2176]{1,0:T(8,128)(2,1)S(1)} %copy-done.51), channel_id=1, source_target_pairs={{0,5},{1,4},{2,7},{3,6},{4,1},{5,0},{6,3},{7,2},{8,13},{9,12},{10,... | collective-permute-start | bytes 417800 | tf_op jit(solution)/shard_map/ppermute | solution.py:27
  32.1 22.2 %collective-permute-start.16 = (bf16[32,2176]{1,0:T(8,128)(2,1)S(1)}, bf16[32,2176]{1,0:T(8,128)(2,1)S(1)}, u32[]{:S(2)}, u32[]{:S(2)}) collective-permute-start(bf16[32,2176]{1,0:T(8,128)(2,1)S(1)} %copy-done.50), channel_id=1, source_target_pairs={{0,6},{1,7},{2,4},{3,5},{4,2},{5,3},{6,0},{7,1},{8,14},{9,15},{10,... | collective-permute-start | bytes 417800 | tf_op jit(solution)/shard_map/ppermute | solution.py:27
  39.4 23.1 %collective-permute-start.17 = (bf16[32,2176]{1,0:T(8,128)(2,1)S(1)}, bf16[32,2176]{1,0:T(8,128)(2,1)S(1)}, u32[]{:S(2)}, u32[]{:S(2)}) collective-permute-start(bf16[32,2176]{1,0:T(8,128)(2,1)S(1)} %copy-done.49), channel_id=1, source_target_pairs={{0,7},{1,6},{2,5},{3,4},{4,3},{5,2},{6,1},{7,0},{8,15},{9,14},{10,... | collective-permute-start | bytes 417800 | tf_op jit(solution)/shard_map/ppermute | solution.py:27
  39.5 27.9 %collective-permute-start.11 = (bf16[32,2176]{1,0:T(8,128)(2,1)S(1)}, bf16[32,2176]{1,0:T(8,128)(2,1)S(1)}, u32[]{:S(2)}, u32[]{:S(2)}) collective-permute-start(bf16[32,2176]{1,0:T(8,128)(2,1)S(1)} %copy-done.48), channel_id=1, source_target_pairs={{0,1},{1,0},{2,3},{3,2},{4,5},{5,4},{6,7},{7,6},{8,9},{9,8},{10,11... | collective-permute-start | bytes 417800 | tf_op jit(solution)/shard_map/ppermute | solution.py:27
  39.8 43.2 %collective-permute-start.3 = (bf16[2,2,128,256]{3,2,1,0:T(8,128)(2,1)}, bf16[2,2,128,256]{3,2,1,0:T(8,128)(2,1)S(1)}, u32[]{:S(2)}, u32[]{:S(2)}) collective-permute-start(bf16[2,2,128,256]{3,2,1,0:T(8,128)(2,1)} %get-tuple-element.75), channel_id=1, source_target_pairs={{0,4},{1,5},{2,6},{3,7},{4,0},{5,1},{6,2},{7,3},{8,12},{9,13},{10,... | collective-permute-start | bytes 786440 | tf_op jit(solution)/shard_map/ppermute | solution.py:27
  62.5 24.6 %collective-permute-start.4 = (bf16[2,2,128,256]{3,2,1,0:T(8,128)(2,1)}, bf16[2,2,128,256]{3,2,1,0:T(8,128)(2,1)S(1)}, u32[]{:S(2)}, u32[]{:S(2)}) collective-permute-start(bf16[2,2,128,256]{3,2,1,0:T(8,128)(2,1)} %get-tuple-element.76), channel_id=1, source_target_pairs={{0,5},{1,4},{2,7},{3,6},{4,1},{5,0},{6,3},{7,2},{8,13},{9,12},{10,... | collective-permute-start | bytes 786440 | tf_op jit(solution)/shard_map/ppermute | solution.py:27
  67.4 22.2 %collective-permute-start.5 = (bf16[2,2,128,256]{3,2,1,0:T(8,128)(2,1)}, bf16[2,2,128,256]{3,2,1,0:T(8,128)(2,1)S(1)}, u32[]{:S(2)}, u32[]{:S(2)}) collective-permute-start(bf16[2,2,128,256]{3,2,1,0:T(8,128)(2,1)} %get-tuple-element.77), channel_id=1, source_target_pairs={{0,6},{1,7},{2,4},{3,5},{4,2},{5,3},{6,0},{7,1},{8,14},{9,15},{10,... | collective-permute-start | bytes 786440 | tf_op jit(solution)/shard_map/ppermute | solution.py:27
  68.3 23.5 %collective-permute-start = (bf16[3,2,128,256]{3,2,1,0:T(8,128)(2,1)}, bf16[3,2,128,256]{3,2,1,0:T(8,128)(2,1)S(1)}, u32[]{:S(2)}, u32[]{:S(2)}) collective-permute-start(bf16[3,2,128,256]{3,2,1,0:T(8,128)(2,1)} %get-tuple-element.72), channel_id=1, source_target_pairs={{0,1},{1,0},{2,3},{3,2},{4,5},{5,4},{6,7},{7,6},{8,9},{9,8},{10,11... | collective-permute-start | bytes 1179656 | tf_op jit(solution)/shard_map/ppermute | solution.py:27
  71.0 25.4 %collective-permute-start.1 = (bf16[3,2,128,256]{3,2,1,0:T(8,128)(2,1)}, bf16[3,2,128,256]{3,2,1,0:T(8,128)(2,1)S(1)}, u32[]{:S(2)}, u32[]{:S(2)}) collective-permute-start(bf16[3,2,128,256]{3,2,1,0:T(8,128)(2,1)} %get-tuple-element.73), channel_id=1, source_target_pairs={{0,2},{1,3},{2,0},{3,1},{4,6},{5,7},{6,4},{7,5},{8,10},{9,11},{10,... | collective-permute-start | bytes 1179656 | tf_op jit(solution)/shard_map/ppermute | solution.py:27
  83.0 25.9 %collective-permute-start.2 = (bf16[3,2,128,256]{3,2,1,0:T(8,128)(2,1)}, bf16[3,2,128,256]{3,2,1,0:T(8,128)(2,1)S(1)}, u32[]{:S(2)}, u32[]{:S(2)}) collective-permute-start(bf16[3,2,128,256]{3,2,1,0:T(8,128)(2,1)} %get-tuple-element.74), channel_id=1, source_target_pairs={{0,3},{1,2},{2,1},{3,0},{4,7},{5,6},{6,5},{7,4},{8,11},{9,10},{10,... | collective-permute-start | bytes 1179656 | tf_op jit(solution)/shard_map/ppermute | solution.py:27
  87.8 32.0 %collective-permute-start.19 = (bf16[128,2048]{1,0:T(8,128)(2,1)}, bf16[128,2048]{1,0:T(8,128)(2,1)S(1)}, u32[]{:S(2)}, u32[]{:S(2)}) collective-permute-start(bf16[128,2048]{1,0:T(8,128)(2,1)} %get-tuple-element.97.refs_5_.refs_3_), channel_id=1, source_target_pairs={{0,8},{8,0},{16,24},{24,16},{1,9},{9,1},{17,25},{25,17},{2,10},{10... | collective-permute-start | bytes 1572872 | tf_op jit(solution)/shard_map/ppermute | solution.py:27
  90.3 31.0 %collective-permute-start.20 = (bf16[128,2048]{1,0:T(8,128)(2,1)}, bf16[128,2048]{1,0:T(8,128)(2,1)S(1)}, u32[]{:S(2)}, u32[]{:S(2)}) collective-permute-start(bf16[128,2048]{1,0:T(8,128)(2,1)} %get-tuple-element.96.refs_4_.refs_2_), channel_id=1, source_target_pairs={{0,16},{8,24},{16,0},{24,8},{1,17},{9,25},{17,1},{25,9},{2,18},{10... | collective-permute-start | bytes 1572872 | tf_op jit(solution)/shard_map/ppermute | solution.py:27
  113.3 36.3 %collective-permute-start.21 = (bf16[128,2048]{1,0:T(8,128)(2,1)S(1)}, bf16[128,2048]{1,0:T(8,128)(2,1)S(1)}, u32[]{:S(2)}, u32[]{:S(2)}) collective-permute-start(bf16[128,2048]{1,0:T(8,128)(2,1)S(1)} %copy-done), channel_id=1, source_target_pairs={{0,16},{8,24},{16,0},{24,8},{1,17},{9,25},{17,1},{25,9},{2,18},{10... | collective-permute-start | bytes 1572872 | tf_op jit(solution)/shard_map/ppermute | solution.py:27
  118.4 31.9 %collective-permute-start.18 = (bf16[128,2048]{1,0:T(8,128)(2,1)S(1)}, bf16[128,2048]{1,0:T(8,128)(2,1)S(1)}, u32[]{:S(2)}, u32[]{:S(2)}) collective-permute-start(bf16[128,2048]{1,0:T(8,128)(2,1)S(1)} %copy-done.1), channel_id=1, source_target_pairs={{0,8},{8,0},{16,24},{24,16},{1,9},{9,1},{17,25},{25,17},{2,10},{10... | collective-permute-start | bytes 1572872 | tf_op jit(solution)/shard_map/ppermute | solution.py:27
  119.8 31.1 %collective-permute-start.23 = (bf16[128,2048]{1,0:T(8,128)(2,1)S(1)}, bf16[128,2048]{1,0:T(8,128)(2,1)S(1)}, u32[]{:S(2)}, u32[]{:S(2)}) collective-permute-start(bf16[128,2048]{1,0:T(8,128)(2,1)S(1)} %collective-permute-done.19.refs_7_.refs_5_), channel_id=1, source_target_pairs={{0,16},{8,24},{16,0},{24,8},{1,17},{9,25},{17,1},{25,9},{2,18},{10... | collective-permute-start | bytes 1572872 | tf_op jit(solution)/shard_map/ppermute | solution.py:27
  121.3 30.9 %collective-permute-start.22 = (bf16[128,2048]{1,0:T(8,128)(2,1)S(1)}, bf16[128,2048]{1,0:T(8,128)(2,1)S(1)}, u32[]{:S(2)}, u32[]{:S(2)}) collective-permute-start(bf16[128,2048]{1,0:T(8,128)(2,1)S(1)} %collective-permute-done.20.refs_8_.refs_6_), channel_id=1, source_target_pairs={{0,8},{8,0},{16,24},{24,16},{1,9},{9,1},{17,25},{25,17},{2,10},{10... | collective-permute-start | bytes 1572872 | tf_op jit(solution)/shard_map/ppermute | solution.py:27
  124.0 23.4 %collective-permute-start.31 = (bf16[128,1024]{1,0:T(8,128)(2,1)}, bf16[128,1024]{1,0:T(8,128)(2,1)}, u32[]{:S(2)}, u32[]{:S(2)}) collective-permute-start(bf16[128,1024]{1,0:T(8,128)(2,1)} %get-tuple-element.119.refs_5_), channel_id=1, source_target_pairs={{0,8},{8,0},{16,24},{24,16},{1,9},{9,1},{17,25},{25,17},{2,10},{10... | collective-permute-start | bytes 786440 | tf_op jit(solution)/shard_map/ppermute | solution.py:27
  150.2 22.4 %collective-permute-start.33 = (bf16[128,1024]{1,0:T(8,128)(2,1)}, bf16[128,1024]{1,0:T(8,128)(2,1)S(1)}, u32[]{:S(2)}, u32[]{:S(2)}) collective-permute-start(bf16[128,1024]{1,0:T(8,128)(2,1)} %get-tuple-element.119.refs_5_), channel_id=1, source_target_pairs={{0,16},{8,24},{16,0},{24,8},{1,17},{9,25},{17,1},{25,9},{2,18},{10... | collective-permute-start | bytes 786440 | tf_op jit(solution)/shard_map/ppermute | solution.py:27
  150.9 22.3 %collective-permute-start.34 = (bf16[128,1024]{1,0:T(8,128)(2,1)}, bf16[128,1024]{1,0:T(8,128)(2,1)S(1)}, u32[]{:S(2)}, u32[]{:S(2)}) collective-permute-start(bf16[128,1024]{1,0:T(8,128)(2,1)} %collective-permute-done.32.refs_8_), channel_id=1, source_target_pairs={{0,8},{8,0},{16,24},{24,16},{1,9},{9,1},{17,25},{25,17},{2,10},{10... | collective-permute-start | bytes 786440 | tf_op jit(solution)/shard_map/ppermute | solution.py:27
  171.4 22.8 %collective-permute-start.27 = (bf16[256,512]{1,0:T(8,128)(2,1)}, bf16[256,512]{1,0:T(8,128)(2,1)S(1)}, u32[]{:S(2)}, u32[]{:S(2)}) collective-permute-start(bf16[256,512]{1,0:T(8,128)(2,1)} %stack_columns.3.refs_4_), channel_id=1, source_target_pairs={{0,8},{8,0},{16,24},{24,16},{1,9},{9,1},{17,25},{25,17},{2,10},{10... | collective-permute-start | bytes 786440 | tf_op jit(solution)/shard_map/ppermute | solution.py:27
  (79 other events, 1373.7 us)

commit v2 on v1

--- a/solution.py
+++ b/solution.py
@@ -11,6 +11,7 @@
 EPS = 1e-06
 LANES = 128
 BLOCKS = 2
+ROOM = 16 << 20
 VMEM = pl.BlockSpec(memory_space=pltpu.VMEM)
 
 
@@ -72,6 +73,7 @@
         out_shape=[jax.ShapeDtypeStruct((groups * cap, tokens), jnp.bfloat16)] + [block] * groups,
         in_specs=[pl.BlockSpec(memory_space=pltpu.SMEM)] + [VMEM] * 3,
         out_specs=[VMEM] * (groups + 1),
+        compiler_params=pltpu.CompilerParams(vmem_limit_bytes=ROOM),
         cost_estimate=cost(2 * groups * cap * tokens * width, 2 * tokens * width * 6),
         name="route",
     )(me, prompt, group_pick.reshape(1, tokens), route_weight.T)
@@ -103,6 +105,7 @@
         out_shape=[shape(3)] * half + [shape(2), shape()] * (groups - half),
         in_specs=[pl.BlockSpec(memory_space=pltpu.SMEM), pl.BlockSpec(memory_space=pl.ANY)] + [VMEM] * 4,
         out_specs=[VMEM] * (2 * groups - half),
+        compiler_params=pltpu.CompilerParams(vmem_limit_bytes=ROOM),
         cost_estimate=cost(4 * size, 6 * size),
         name="rounding",
     )(me, after, gain.reshape(1, -1), gate, up, down)
@@ -153,6 +156,7 @@
         in_specs=[pl.BlockSpec(memory_space=pltpu.SMEM)] + [VMEM] * sum(sizes),
         out_specs=[pl.BlockSpec(memory_space=pl.ANY)] * 3,
         scratch_shapes=[pltpu.SemaphoreType.DMA((3, count))],
+        compiler_params=pltpu.CompilerParams(vmem_limit_bytes=ROOM),
         cost_estimate=cost(4 * size, 4 * size),
         name="joining",
     )(me, *near, *pairs, *downs)
@@ -176,6 +180,7 @@
         ],
         in_specs=[VMEM] * count,
         out_specs=[VMEM] * 2,
+        compiler_params=pltpu.CompilerParams(vmem_limit_bytes=ROOM),
         cost_estimate=cost(count * cap * width, 4 * count * cap * width),
         name="stack_rows",
     )(*blocks)
@@ -185,21 +190,34 @@
     count = len(blocks)
     experts, units, part = blocks[0].shape[-3:]
     rows = experts * units // pieces
+    moved = part % LANES == 0
 
     def kernel(*refs):
-        ins, outs = refs[:count], refs[count:]
+        ins, outs, sems = refs[:count], refs[count:-1], refs[-1]
+        copies = []
         for d, block in enumerate(ins):
             piece = block.at[2] if len(block.shape) == 4 else block
             for x in range(experts):
                 row = x * units % rows
-                outs[x * units // rows][row : row + units, d * part : (d + 1) * part] = piece[x]
+                spot = (slice(row, row + units), slice(d * part, (d + 1) * part))
+                out = outs[x * units // rows]
+                if moved:
+                    copies.append(pltpu.make_async_copy(piece.at[x], out.at[spot], sems.at[d, x]))
+                else:
+                    out[spot] = piece[x]
+        for copy in copies:
+            copy.start()
+        for copy in copies:
+            copy.wait()
 
     size = count * experts * units * part
     return pl.pallas_call(
         kernel,
         out_shape=[jax.ShapeDtypeStruct((rows, count * part), jnp.bfloat16)] * pieces,
-        in_specs=[VMEM] * count,
+        in_specs=[pl.BlockSpec(memory_space=pl.ANY) if moved else VMEM] * count,
         out_specs=[VMEM] * pieces,
+        scratch_shapes=[pltpu.SemaphoreType.DMA((count, experts))],
+        compiler_params=pltpu.CompilerParams(vmem_limit_bytes=ROOM),
         cost_estimate=cost(size, 4 * size),
         name="stack_columns",
     )(*blocks)
@@ -230,21 +248,26 @@
     place = lax.shift_right_logical(me_ref[0] ^ first, parts.bit_length() - 1)
     columns = pl.ds(pl.multiple_of(place * width, width), width)
     slots = rows[0].shape[0]
-    spot = lambda b: rows_ref.at[b * slots // rows_ref.shape[1], pl.ds(b * slots % rows_ref.shape[1], slots)]
+    row_spot = lambda b: rows_ref.at[b * slots // rows_ref.shape[1], pl.ds(b * slots % rows_ref.shape[1], slots)]
     copies = [
-        pltpu.make_async_copy(ref.at[:, columns], spot(b), sems.at[0, b]) for b, ref in enumerate(rows)
+        pltpu.make_async_copy(ref.at[:, columns], row_spot(b), sems.at[0, b]) for b, ref in enumerate(rows)
     ]
     copies += [
         pltpu.make_async_copy(ref, sums_ref.at[b], sems.at[1, b]) for b, ref in enumerate(before)
     ]
-    for copy in copies:
-        copy.start()
+    fills = []
     for d, piece in enumerate(pieces):
         start = pl.multiple_of(((me_ref[0] & (len(pieces) - 1)) ^ d) * part, part)
         for which in range(2):
             for x in range(experts):
                 row = which * both + x * units
-                matrix_ref[row : row + units, pl.ds(start, part)] = piece[which, x]
+                spot = matrix_ref.at[row : row + units, pl.ds(start, part)]
+                sem = sems.at[2, (d * 2 + which) * experts + x]
+                fills.append(pltpu.make_async_copy(piece.at[which, x], spot, sem))
+    for copy in fills + copies:
+        copy.start()
+    for copy in fills:
+        copy.wait()
     group = rows_ref.shape[1] // slots
     for m in range(rows_ref.shape[0]):
         mine = range(m * group, (m + 1) * group)
@@ -284,15 +307,15 @@
         functools.partial(active_kernel, first, parts, counts),
         out_shape=outs,
         in_specs=[pl.BlockSpec(memory_space=pltpu.SMEM)]
-        + [VMEM] * len(pieces)
-        + [pl.BlockSpec(memory_space=pl.ANY)] * (count + len(before)),
+        + [pl.BlockSpec(memory_space=pl.ANY)] * (len(pieces) + count + len(before)),
         out_specs=[VMEM] * len(outs),
         scratch_shapes=[
             pltpu.VMEM((2 * both, width), jnp.bfloat16),
             pltpu.VMEM((BLOCKS, count * slots // BLOCKS, width), jnp.bfloat16),
             pltpu.VMEM((max(1, len(before)), slots, 2 * both), jnp.float32),
-            pltpu.SemaphoreType.DMA((2, count)),
+            pltpu.SemaphoreType.DMA((3, max(count, 2 * experts * len(pieces)))),
         ],
+        compiler_params=pltpu.CompilerParams(vmem_limit_bytes=ROOM),
         cost_estimate=cost(4 * count * slots * both * width, 2 * count * slots * width),
         name="active",
     )(me, *pieces, *rows, *before)
@@ -342,6 +365,7 @@
         out_shape=[out(d) for d in range(groups)],
         in_specs=[VMEM] * (2 + members + len(flat) + len(kept)),
         out_specs=[VMEM] * groups,
+        compiler_params=pltpu.CompilerParams(vmem_limit_bytes=ROOM),
         cost_estimate=cost(2 * slots * size, 2 * size),
         name="mixing",
     )(*weights, *hiddens, *flat, *kept)
@@ -390,6 +414,7 @@
         in_specs=[pl.BlockSpec(memory_space=pltpu.SMEM)] + [VMEM] * (1 + len(flat)),
         out_specs=VMEM,
         scratch_shapes=[pltpu.VMEM((slots, width), jnp.bfloat16)],
+        compiler_params=pltpu.CompilerParams(vmem_limit_bytes=ROOM),
         cost_estimate=cost(2 * slots * tokens * width, 2 * slots * width),
         name="finish",
     )(me, placing, *flat)

time: 226 us -> 215 us (0.951)
  Pallas kernels: 44.2 us -> 11.8 us
  waiting for transfers between devices: 82.6 us -> 101 us
  local copies, waits for them, and re-layouts: 4.53 us -> 7.79 us
    ppermute x50, waiting for transfers between devices: 82.6 us -> 101 us  [swap(): return lax.ppermute(value, axis, [(i, i ^ distance) for i in range(count)])]
    pallas_call x3, Pallas kernels: 14.3 us -> 6.03 us  [active_units(): pl.pallas_call(functools.partial(active_kernel, first, parts, counts), ou...]
    pallas_call x3, Pallas kernels: 5.57 us -> 0.27 us  [stacked_columns(): pl.pallas_call(kernel, out_shape=[jax.ShapeDtypeStruct((rows, count * par...]
    pallas_call x2, Pallas kernels: 6.71 us -> 1.46 us  [mixed_rows(): pl.pallas_call(functools.partial(mix_kernel, members, experts, pieces, le...]
    pallas_call x1, Pallas kernels: 4.9 us -> 0.31 us  [rounded(): pl.pallas_call(kernel, out_shape=[shape(3)] * half + [shape(2), shape()]...]
    pallas_call x2, Pallas kernels: 3.94 us -> 0.08 us  [stacked_rows(): pl.pallas_call(functools.partial(stack_rows_kernel, width), out_shape=[ja...]
    unnamed x106 -> x14, local copies, waits for them, and re-layouts: 4.53 us -> 7.79 us
  transfers between devices with their start and end apart: 50 -> 50, of which waited for: 14 -> 19; matrix products, arithmetic and copies ran while one was open for 0% -> 0% of each run, Pallas kernels for 15% -> 5%
where the time goes in v2:
time: 215 us; the launch traced here: 214 us
  waiting for transfers between devices  101 us (47%)
  starting transfers between devices  92 us (43%)
  Pallas kernels  11.8 us (5%)
  local copies, waits for them, and re-layouts  7.79 us (4%)
    ppermute x50, waiting for transfers between devices, swap(): return lax.ppermute(value, axis, [(i, i ^ distance) for i in range(count)])  101 us
    ppermute x50, starting transfers between devices, swap(): return lax.ppermute(value, axis, [(i, i ^ distance) for i in range(count)])  92 us
    unnamed x14, local copies, waits for them, and re-layouts  7.79 us
    pallas_call x3, Pallas kernels, active_units(): pl.pallas_call(functools.partial(active_kernel, first, parts, counts), ou...  6.03 us
  transfers between devices with their start and end apart: 50, of which 19 were waited for; matrix products, arithmetic and copies ran while one was open for 0% of the time, Pallas kernels for 5%

profile of v2, /device:TPU:0, one launch (start us, length us, event | category | flops | bytes accessed | tf_op | source)
XLA Modules:
  0.0 213.7 jit_solution(11287622241423376311)
XLA Ops:
  9.4 4.1 %collective-permute-start.7 = (bf16[2,128,256]{2,1,0:T(8,128)(2,1)S(1)}, bf16[2,128,256]{2,1,0:T(8,128)(2,1)S(1)}, u32[]{:S(2)}, u32[]{:S(2)}) collective-permute-start(bf16[2,128,256]{2,1,0:T(8,128)(2,1)S(1)} %get-tuple-element.79), channel_id=1, source_target_pairs={{0,4},{1,5},{2,6},{3,7},{4,0},{5,1},{6,2},{7,3},{8,12},{9,13},{10,... | collective-permute-start | bytes 393224 | tf_op jit(solution)/shard_map/ppermute | solution.py:28
  17.2 2.5 %collective-permute-start.9 = (bf16[2,128,256]{2,1,0:T(8,128)(2,1)S(1)}, bf16[2,128,256]{2,1,0:T(8,128)(2,1)S(1)}, u32[]{:S(2)}, u32[]{:S(2)}) collective-permute-start(bf16[2,128,256]{2,1,0:T(8,128)(2,1)S(1)} %get-tuple-element.81), channel_id=1, source_target_pairs={{0,6},{1,7},{2,4},{3,5},{4,2},{5,3},{6,0},{7,1},{8,14},{9,15},{10,... | collective-permute-start | bytes 393224 | tf_op jit(solution)/shard_map/ppermute | solution.py:28
  19.7 12.4 %collective-permute-done.7.refs_8_.refs_0_ = bf16[2,128,256]{2,1,0:T(8,128)(2,1)S(1)} collective-permute-done((bf16[2,128,256]{2,1,0:T(8,128)(2,1)S(1)}, bf16[2,128,256]{2,1,0:T(8,128)(2,1)S(1)}, u32[]{:S(2)}, u32[]{:S(2)}) %collective-permute-start.7) | collective-permute-done | bytes 131104 | tf_op jit(solution)/shard_map/ppermute | solution.py:28
  33.2 7.3 %collective-permute-start.16 = (bf16[32,2176]{1,0:T(8,128)(2,1)S(1)}, bf16[32,2176]{1,0:T(8,128)(2,1)S(1)}, u32[]{:S(2)}, u32[]{:S(2)}) collective-permute-start(bf16[32,2176]{1,0:T(8,128)(2,1)S(1)} %get-tuple-element.93), channel_id=1, source_target_pairs={{0,6},{1,7},{2,4},{3,5},{4,2},{5,3},{6,0},{7,1},{8,14},{9,15},{10,... | collective-permute-start | bytes 417800 | tf_op jit(solution)/shard_map/ppermute | solution.py:28
  40.9 13.5 %collective-permute-start.3 = (bf16[2,2,128,256]{3,2,1,0:T(8,128)(2,1)S(1)}, bf16[2,2,128,256]{3,2,1,0:T(8,128)(2,1)S(1)}, u32[]{:S(2)}, u32[]{:S(2)}) collective-permute-start(bf16[2,2,128,256]{3,2,1,0:T(8,128)(2,1)S(1)} %get-tuple-element.75), channel_id=1, source_target_pairs={{0,4},{1,5},{2,6},{3,7},{4,0},{5,1},{6,2},{7,3},{8,12},{9,13},{10,... | collective-permute-start | bytes 786440 | tf_op jit(solution)/shard_map/ppermute | solution.py:28
  55.4 8.1 %collective-permute-start.13 = (bf16[32,2176]{1,0:T(8,128)(2,1)S(1)}, bf16[32,2176]{1,0:T(8,128)(2,1)S(1)}, u32[]{:S(2)}, u32[]{:S(2)}) collective-permute-start(bf16[32,2176]{1,0:T(8,128)(2,1)S(1)} %get-tuple-element.89), channel_id=1, source_target_pairs={{0,3},{1,2},{2,1},{3,0},{4,7},{5,6},{6,5},{7,4},{8,11},{9,10},{10,... | collective-permute-start | bytes 417800 | tf_op jit(solution)/shard_map/ppermute | solution.py:28
  63.5 4.9 %collective-permute-start.4 = (bf16[2,2,128,256]{3,2,1,0:T(8,128)(2,1)S(1)}, bf16[2,2,128,256]{3,2,1,0:T(8,128)(2,1)S(1)}, u32[]{:S(2)}, u32[]{:S(2)}) collective-permute-start(bf16[2,2,128,256]{3,2,1,0:T(8,128)(2,1)S(1)} %get-tuple-element.76), channel_id=1, source_target_pairs={{0,5},{1,4},{2,7},{3,6},{4,1},{5,0},{6,3},{7,2},{8,13},{9,12},{10,... | collective-permute-start | bytes 786440 | tf_op jit(solution)/shard_map/ppermute | solution.py:28
  69.4 2.6 %collective-permute-done.13.refs_3_ = bf16[32,2176]{1,0:T(8,128)(2,1)S(1)} collective-permute-done((bf16[32,2176]{1,0:T(8,128)(2,1)S(1)}, bf16[32,2176]{1,0:T(8,128)(2,1)S(1)}, u32[]{:S(2)}, u32[]{:S(2)}) %collective-permute-start.13) | collective-permute-done | bytes 139296 | tf_op jit(solution)/shard_map/ppermute | solution.py:28
  72.5 11.5 %collective-permute-done.3.refs_4_.refs_0_ = bf16[2,2,128,256]{3,2,1,0:T(8,128)(2,1)S(1)} collective-permute-done((bf16[2,2,128,256]{3,2,1,0:T(8,128)(2,1)S(1)}, bf16[2,2,128,256]{3,2,1,0:T(8,128)(2,1)S(1)}, u32[]{:S(2)}, u32[]{:S(2)}) %collective-permute-start.3) | collective-permute-done | bytes 262176 | tf_op jit(solution)/shard_map/ppermute | solution.py:28
  84.1 3.8 %collective-permute-done.4.refs_5_.refs_1_ = bf16[2,2,128,256]{3,2,1,0:T(8,128)(2,1)S(1)} collective-permute-done((bf16[2,2,128,256]{3,2,1,0:T(8,128)(2,1)S(1)}, bf16[2,2,128,256]{3,2,1,0:T(8,128)(2,1)S(1)}, u32[]{:S(2)}, u32[]{:S(2)}) %collective-permute-start.4) | collective-permute-done | bytes 262176 | tf_op jit(solution)/shard_map/ppermute | solution.py:28
  90.7 3.6 %collective-permute-start.6 = (bf16[2,2,128,256]{3,2,1,0:T(8,128)(2,1)S(1)}, bf16[2,2,128,256]{3,2,1,0:T(8,128)(2,1)S(1)}, u32[]{:S(2)}, u32[]{:S(2)}) collective-permute-start(bf16[2,2,128,256]{3,2,1,0:T(8,128)(2,1)S(1)} %get-tuple-element.78), channel_id=1, source_target_pairs={{0,7},{1,6},{2,5},{3,4},{4,3},{5,2},{6,1},{7,0},{8,15},{9,14},{10,... | collective-permute-start | bytes 786440 | tf_op jit(solution)/shard_map/ppermute | solution.py:28
  96.9 12.8 %collective-permute-done.2.refs_3_ = bf16[3,2,128,256]{3,2,1,0:T(8,128)(2,1)S(1)} collective-permute-done((bf16[3,2,128,256]{3,2,1,0:T(8,128)(2,1)S(1)}, bf16[3,2,128,256]{3,2,1,0:T(8,128)(2,1)S(1)}, u32[]{:S(2)}, u32[]{:S(2)}) %collective-permute-start.2) | collective-permute-done | bytes 393248 | tf_op jit(solution)/shard_map/ppermute | solution.py:28
  113.4 5.4 %collective-permute-done.37.refs_14_ = bf16[256,512]{1,0:T(8,128)(2,1)S(1)} collective-permute-done((bf16[256,512]{1,0:T(8,128)(2,1)S(1)}, bf16[256,512]{1,0:T(8,128)(2,1)S(1)}, u32[]{:S(2)}, u32[]{:S(2)}) %collective-permute-start.37) | collective-permute-done | bytes 262176 | tf_op jit(solution)/shard_map/ppermute | solution.py:28
  125.9 21.8 %collective-permute-done.31.refs_7_ = bf16[128,1024]{1,0:T(8,128)(2,1)S(1)} collective-permute-done((bf16[128,1024]{1,0:T(8,128)(2,1)S(1)}, bf16[128,1024]{1,0:T(8,128)(2,1)S(1)}, u32[]{:S(2)}, u32[]{:S(2)}) %collective-permute-start.31) | collective-permute-done | bytes 262176 | tf_op jit(solution)/shard_map/ppermute | solution.py:28
  147.7 2.5 %collective-permute-start.38 = (bf16[256,512]{1,0:T(8,128)(2,1)S(1)}, bf16[256,512]{1,0:T(8,128)(2,1)S(1)}, u32[]{:S(2)}, u32[]{:S(2)}) collective-permute-start(bf16[256,512]{1,0:T(8,128)(2,1)S(1)} %stack_columns.5.refs_12_), channel_id=1, source_target_pairs={{0,24},{8,16},{16,8},{24,0},{1,25},{9,17},{17,9},{25,1},{2,26},{10... | collective-permute-start | bytes 786440 | tf_op jit(solution)/shard_map/ppermute | solution.py:28
  160.9 2.5 %collective-permute-done.30.refs_6_ = bf16[128,1024]{1,0:T(8,128)(2,1)S(1)} collective-permute-done((bf16[128,1024]{1,0:T(8,128)(2,1)S(1)}, bf16[128,1024]{1,0:T(8,128)(2,1)S(1)}, u32[]{:S(2)}, u32[]{:S(2)}) %collective-permute-start.30) | collective-permute-done | bytes 262176 | tf_op jit(solution)/shard_map/ppermute | solution.py:28
  165.3 3.6 %collective-permute-done.34.refs_10_ = bf16[128,1024]{1,0:T(8,128)(2,1)S(1)} collective-permute-done((bf16[128,1024]{1,0:T(8,128)(2,1)S(1)}, bf16[128,1024]{1,0:T(8,128)(2,1)S(1)}, u32[]{:S(2)}, u32[]{:S(2)}) %collective-permute-start.34) | collective-permute-done | bytes 262176 | tf_op jit(solution)/shard_map/ppermute | solution.py:28
  173.2 4.3 %collective-permute-done.25.refs_2_ = bf16[256,256]{1,0:T(8,128)(2,1)S(1)} collective-permute-done((bf16[256,256]{1,0:T(8,128)(2,1)S(1)}, bf16[256,256]{1,0:T(8,128)(2,1)S(1)}, u32[]{:S(2)}, u32[]{:S(2)}) %collective-permute-start.25) | collective-permute-done | bytes 131104 | tf_op jit(solution)/shard_map/ppermute | solution.py:28
  177.5 4.8 %collective-permute-done.26.refs_3_ = bf16[256,256]{1,0:T(8,128)(2,1)S(1)} collective-permute-done((bf16[256,256]{1,0:T(8,128)(2,1)S(1)}, bf16[256,256]{1,0:T(8,128)(2,1)S(1)}, u32[]{:S(2)}, u32[]{:S(2)}) %collective-permute-start.26) | collective-permute-done | bytes 131104 | tf_op jit(solution)/shard_map/ppermute | solution.py:28
  189.2 3.8 %collective-permute-start.47 = (bf16[32,512]{1,0:T(8,128)(2,1)S(1)}, bf16[32,512]{1,0:T(8,128)(2,1)S(1)}, u32[]{:S(2)}, u32[]{:S(2)}) collective-permute-start(bf16[32,512]{1,0:T(8,128)(2,1)S(1)} %get-tuple-element.133), channel_id=1, source_target_pairs={{0,6},{1,7},{2,4},{3,5},{4,2},{5,3},{6,0},{7,1},{8,14},{9,15},{10,... | collective-permute-start | bytes 98312 | tf_op jit(solution)/shard_map/ppermute | solution.py:28
  193.0 4.0 %collective-permute-done.43.refs_5_ = bf16[32,512]{1,0:T(8,128)(2,1)S(1)} collective-permute-done((bf16[32,512]{1,0:T(8,128)(2,1)S(1)}, bf16[32,512]{1,0:T(8,128)(2,1)S(1)}, u32[]{:S(2)}, u32[]{:S(2)}) %collective-permute-start.43) | collective-permute-done | bytes 32800 | tf_op jit(solution)/shard_map/ppermute | solution.py:28
  197.6 2.8 %collective-permute-start.39 = (bf16[32,2048]{1,0:T(8,128)(2,1)S(1)}, bf16[32,2048]{1,0:T(8,128)(2,1)S(1)}, u32[]{:S(2)}, u32[]{:S(2)}) collective-permute-start(bf16[32,2048]{1,0:T(8,128)(2,1)S(1)} %get-tuple-element.125), channel_id=1, source_target_pairs={{0,1},{1,0},{2,3},{3,2},{4,5},{5,4},{6,7},{7,6},{8,9},{9,8},{10,11... | collective-permute-start | bytes 393224 | tf_op jit(solution)/shard_map/ppermute | solution.py:28
  202.4 3.2 %collective-permute-start.46 = (bf16[32,1536]{1,0:T(8,128)(2,1)S(1)}, bf16[32,1536]{1,0:T(8,128)(2,1)S(1)}, u32[]{:S(2)}, u32[]{:S(2)}) collective-permute-start(bf16[32,1536]{1,0:T(8,128)(2,1)S(1)} %get-tuple-element.132), channel_id=1, source_target_pairs={{0,6},{1,7},{2,4},{3,5},{4,2},{5,3},{6,0},{7,1},{8,14},{9,15},{10,... | collective-permute-start | bytes 294920 | tf_op jit(solution)/shard_map/ppermute | solution.py:28
  207.6 3.1 %collective-permute-done.46.refs_8_ = bf16[32,1536]{1,0:T(8,128)(2,1)S(1)} collective-permute-done((bf16[32,1536]{1,0:T(8,128)(2,1)S(1)}, bf16[32,1536]{1,0:T(8,128)(2,1)S(1)}, u32[]{:S(2)}, u32[]{:S(2)}) %collective-permute-start.46) | collective-permute-done | bytes 98336 | tf_op jit(solution)/shard_map/ppermute | solution.py:28
  (104 shorter events, 63.9 us)
Async XLA Ops:
  9.4 22.7 %collective-permute-start.7 = (bf16[2,128,256]{2,1,0:T(8,128)(2,1)S(1)}, bf16[2,128,256]{2,1,0:T(8,128)(2,1)S(1)}, u32[]{:S(2)}, u32[]{:S(2)}) collective-permute-start(bf16[2,128,256]{2,1,0:T(8,128)(2,1)S(1)} %get-tuple-element.79), channel_id=1, source_target_pairs={{0,4},{1,5},{2,6},{3,7},{4,0},{5,1},{6,2},{7,3},{8,12},{9,13},{10,... | collective-permute-start | bytes 393224 | tf_op jit(solution)/shard_map/ppermute | solution.py:28
  13.5 27.3 %collective-permute-start.14 = (bf16[32,2176]{1,0:T(8,128)(2,1)S(1)}, bf16[32,2176]{1,0:T(8,128)(2,1)S(1)}, u32[]{:S(2)}, u32[]{:S(2)}) collective-permute-start(bf16[32,2176]{1,0:T(8,128)(2,1)S(1)} %get-tuple-element.91), channel_id=1, source_target_pairs={{0,4},{1,5},{2,6},{3,7},{4,0},{5,1},{6,2},{7,3},{8,12},{9,13},{10,... | collective-permute-start | bytes 417800 | tf_op jit(solution)/shard_map/ppermute | solution.py:28
  15.6 24.9 %collective-permute-start.10 = (bf16[2,128,256]{2,1,0:T(8,128)(2,1)S(1)}, bf16[2,128,256]{2,1,0:T(8,128)(2,1)S(1)}, u32[]{:S(2)}, u32[]{:S(2)}) collective-permute-start(bf16[2,128,256]{2,1,0:T(8,128)(2,1)S(1)} %get-tuple-element.82), channel_id=1, source_target_pairs={{0,7},{1,6},{2,5},{3,4},{4,3},{5,2},{6,1},{7,0},{8,15},{9,14},{10,... | collective-permute-start | bytes 393224 | tf_op jit(solution)/shard_map/ppermute | solution.py:28
  17.2 23.3 %collective-permute-start.9 = (bf16[2,128,256]{2,1,0:T(8,128)(2,1)S(1)}, bf16[2,128,256]{2,1,0:T(8,128)(2,1)S(1)}, u32[]{:S(2)}, u32[]{:S(2)}) collective-permute-start(bf16[2,128,256]{2,1,0:T(8,128)(2,1)S(1)} %get-tuple-element.81), channel_id=1, source_target_pairs={{0,6},{1,7},{2,4},{3,5},{4,2},{5,3},{6,0},{7,1},{8,14},{9,15},{10,... | collective-permute-start | bytes 393224 | tf_op jit(solution)/shard_map/ppermute | solution.py:28
  32.1 22.3 %collective-permute-start.15 = (bf16[32,2176]{1,0:T(8,128)(2,1)S(1)}, bf16[32,2176]{1,0:T(8,128)(2,1)S(1)}, u32[]{:S(2)}, u32[]{:S(2)}) collective-permute-start(bf16[32,2176]{1,0:T(8,128)(2,1)S(1)} %get-tuple-element.92), channel_id=1, source_target_pairs={{0,5},{1,4},{2,7},{3,6},{4,1},{5,0},{6,3},{7,2},{8,13},{9,12},{10,... | collective-permute-start | bytes 417800 | tf_op jit(solution)/shard_map/ppermute | solution.py:28
  33.2 22.2 %collective-permute-start.16 = (bf16[32,2176]{1,0:T(8,128)(2,1)S(1)}, bf16[32,2176]{1,0:T(8,128)(2,1)S(1)}, u32[]{:S(2)}, u32[]{:S(2)}) collective-permute-start(bf16[32,2176]{1,0:T(8,128)(2,1)S(1)} %get-tuple-element.93), channel_id=1, source_target_pairs={{0,6},{1,7},{2,4},{3,5},{4,2},{5,3},{6,0},{7,1},{8,14},{9,15},{10,... | collective-permute-start | bytes 417800 | tf_op jit(solution)/shard_map/ppermute | solution.py:28
  40.5 23.1 %collective-permute-start.17 = (bf16[32,2176]{1,0:T(8,128)(2,1)S(1)}, bf16[32,2176]{1,0:T(8,128)(2,1)S(1)}, u32[]{:S(2)}, u32[]{:S(2)}) collective-permute-start(bf16[32,2176]{1,0:T(8,128)(2,1)S(1)} %get-tuple-element.94), channel_id=1, source_target_pairs={{0,7},{1,6},{2,5},{3,4},{4,3},{5,2},{6,1},{7,0},{8,15},{9,14},{10,... | collective-permute-start | bytes 417800 | tf_op jit(solution)/shard_map/ppermute | solution.py:28
  40.5 28.0 %collective-permute-start.11 = (bf16[32,2176]{1,0:T(8,128)(2,1)S(1)}, bf16[32,2176]{1,0:T(8,128)(2,1)S(1)}, u32[]{:S(2)}, u32[]{:S(2)}) collective-permute-start(bf16[32,2176]{1,0:T(8,128)(2,1)S(1)} %get-tuple-element.87), channel_id=1, source_target_pairs={{0,1},{1,0},{2,3},{3,2},{4,5},{5,4},{6,7},{7,6},{8,9},{9,8},{10,11... | collective-permute-start | bytes 417800 | tf_op jit(solution)/shard_map/ppermute | solution.py:28
  40.9 43.2 %collective-permute-start.3 = (bf16[2,2,128,256]{3,2,1,0:T(8,128)(2,1)S(1)}, bf16[2,2,128,256]{3,2,1,0:T(8,128)(2,1)S(1)}, u32[]{:S(2)}, u32[]{:S(2)}) collective-permute-start(bf16[2,2,128,256]{3,2,1,0:T(8,128)(2,1)S(1)} %get-tuple-element.75), channel_id=1, source_target_pairs={{0,4},{1,5},{2,6},{3,7},{4,0},{5,1},{6,2},{7,3},{8,12},{9,13},{10,... | collective-permute-start | bytes 786440 | tf_op jit(solution)/shard_map/ppermute | solution.py:28
  63.5 24.4 %collective-permute-start.4 = (bf16[2,2,128,256]{3,2,1,0:T(8,128)(2,1)S(1)}, bf16[2,2,128,256]{3,2,1,0:T(8,128)(2,1)S(1)}, u32[]{:S(2)}, u32[]{:S(2)}) collective-permute-start(bf16[2,2,128,256]{3,2,1,0:T(8,128)(2,1)S(1)} %get-tuple-element.76), channel_id=1, source_target_pairs={{0,5},{1,4},{2,7},{3,6},{4,1},{5,0},{6,3},{7,2},{8,13},{9,12},{10,... | collective-permute-start | bytes 786440 | tf_op jit(solution)/shard_map/ppermute | solution.py:28
  68.4 20.8 %collective-permute-start.5 = (bf16[2,2,128,256]{3,2,1,0:T(8,128)(2,1)S(1)}, bf16[2,2,128,256]{3,2,1,0:T(8,128)(2,1)S(1)}, u32[]{:S(2)}, u32[]{:S(2)}) collective-permute-start(bf16[2,2,128,256]{3,2,1,0:T(8,128)(2,1)S(1)} %get-tuple-element.77), channel_id=1, source_target_pairs={{0,6},{1,7},{2,4},{3,5},{4,2},{5,3},{6,0},{7,1},{8,14},{9,15},{10,... | collective-permute-start | bytes 786440 | tf_op jit(solution)/shard_map/ppermute | solution.py:28
  69.4 21.4 %collective-permute-start = (bf16[3,2,128,256]{3,2,1,0:T(8,128)(2,1)S(1)}, bf16[3,2,128,256]{3,2,1,0:T(8,128)(2,1)S(1)}, u32[]{:S(2)}, u32[]{:S(2)}) collective-permute-start(bf16[3,2,128,256]{3,2,1,0:T(8,128)(2,1)S(1)} %get-tuple-element.72), channel_id=1, source_target_pairs={{0,1},{1,0},{2,3},{3,2},{4,5},{5,4},{6,7},{7,6},{8,9},{9,8},{10,11... | collective-permute-start | bytes 1179656 | tf_op jit(solution)/shard_map/ppermute | solution.py:28
  72.0 23.5 %collective-permute-start.1 = (bf16[3,2,128,256]{3,2,1,0:T(8,128)(2,1)S(1)}, bf16[3,2,128,256]{3,2,1,0:T(8,128)(2,1)S(1)}, u32[]{:S(2)}, u32[]{:S(2)}) collective-permute-start(bf16[3,2,128,256]{3,2,1,0:T(8,128)(2,1)S(1)} %get-tuple-element.73), channel_id=1, source_target_pairs={{0,2},{1,3},{2,0},{3,1},{4,6},{5,7},{6,4},{7,5},{8,10},{9,11},{10,... | collective-permute-start | bytes 1179656 | tf_op jit(solution)/shard_map/ppermute | solution.py:28
  84.0 25.7 %collective-permute-start.2 = (bf16[3,2,128,256]{3,2,1,0:T(8,128)(2,1)S(1)}, bf16[3,2,128,256]{3,2,1,0:T(8,128)(2,1)S(1)}, u32[]{:S(2)}, u32[]{:S(2)}) collective-permute-start(bf16[3,2,128,256]{3,2,1,0:T(8,128)(2,1)S(1)} %get-tuple-element.74), channel_id=1, source_target_pairs={{0,3},{1,2},{2,1},{3,0},{4,7},{5,6},{6,5},{7,4},{8,11},{9,10},{10,... | collective-permute-start | bytes 1179656 | tf_op jit(solution)/shard_map/ppermute | solution.py:28
  87.9 32.4 %collective-permute-start.19 = (bf16[128,2048]{1,0:T(8,128)(2,1)S(1)}, bf16[128,2048]{1,0:T(8,128)(2,1)S(1)}, u32[]{:S(2)}, u32[]{:S(2)}) collective-permute-start(bf16[128,2048]{1,0:T(8,128)(2,1)S(1)} %get-tuple-element.97.refs_5_.refs_3_), channel_id=1, source_target_pairs={{0,8},{8,0},{16,24},{24,16},{1,9},{9,1},{17,25},{25,17},{2,10},{10... | collective-permute-start | bytes 1572872 | tf_op jit(solution)/shard_map/ppermute | solution.py:28
  89.2 32.6 %collective-permute-start.20 = (bf16[128,2048]{1,0:T(8,128)(2,1)S(1)}, bf16[128,2048]{1,0:T(8,128)(2,1)S(1)}, u32[]{:S(2)}, u32[]{:S(2)}) collective-permute-start(bf16[128,2048]{1,0:T(8,128)(2,1)S(1)} %get-tuple-element.96.refs_4_.refs_2_), channel_id=1, source_target_pairs={{0,16},{8,24},{16,0},{24,8},{1,17},{9,25},{17,1},{25,9},{2,18},{10... | collective-permute-start | bytes 1572872 | tf_op jit(solution)/shard_map/ppermute | solution.py:28
  90.7 20.6 %collective-permute-start.6 = (bf16[2,2,128,256]{3,2,1,0:T(8,128)(2,1)S(1)}, bf16[2,2,128,256]{3,2,1,0:T(8,128)(2,1)S(1)}, u32[]{:S(2)}, u32[]{:S(2)}) collective-permute-start(bf16[2,2,128,256]{3,2,1,0:T(8,128)(2,1)S(1)} %get-tuple-element.78), channel_id=1, source_target_pairs={{0,7},{1,6},{2,5},{3,4},{4,3},{5,2},{6,1},{7,0},{8,15},{9,14},{10,... | collective-permute-start | bytes 786440 | tf_op jit(solution)/shard_map/ppermute | solution.py:28
  111.9 38.3 %collective-permute-start.21 = (bf16[128,2048]{1,0:T(8,128)(2,1)S(1)}, bf16[128,2048]{1,0:T(8,128)(2,1)S(1)}, u32[]{:S(2)}, u32[]{:S(2)}) collective-permute-start(bf16[128,2048]{1,0:T(8,128)(2,1)S(1)} %get-tuple-element.97.refs_5_.refs_3_), channel_id=1, source_target_pairs={{0,16},{8,24},{16,0},{24,8},{1,17},{9,25},{17,1},{25,9},{2,18},{10... | collective-permute-start | bytes 1572872 | tf_op jit(solution)/shard_map/ppermute | solution.py:28
  118.9 31.7 %collective-permute-start.18 = (bf16[128,2048]{1,0:T(8,128)(2,1)S(1)}, bf16[128,2048]{1,0:T(8,128)(2,1)S(1)}, u32[]{:S(2)}, u32[]{:S(2)}) collective-permute-start(bf16[128,2048]{1,0:T(8,128)(2,1)S(1)} %get-tuple-element.96.refs_4_.refs_2_), channel_id=1, source_target_pairs={{0,8},{8,0},{16,24},{24,16},{1,9},{9,1},{17,25},{25,17},{2,10},{10... | collective-permute-start | bytes 1572872 | tf_op jit(solution)/shard_map/ppermute | solution.py:28
  120.3 30.9 %collective-permute-start.23 = (bf16[128,2048]{1,0:T(8,128)(2,1)S(1)}, bf16[128,2048]{1,0:T(8,128)(2,1)S(1)}, u32[]{:S(2)}, u32[]{:S(2)}) collective-permute-start(bf16[128,2048]{1,0:T(8,128)(2,1)S(1)} %collective-permute-done.19.refs_7_.refs_5_), channel_id=1, source_target_pairs={{0,16},{8,24},{16,0},{24,8},{1,17},{9,25},{17,1},{25,9},{2,18},{10... | collective-permute-start | bytes 1572872 | tf_op jit(solution)/shard_map/ppermute | solution.py:28
  121.8 30.8 %collective-permute-start.22 = (bf16[128,2048]{1,0:T(8,128)(2,1)S(1)}, bf16[128,2048]{1,0:T(8,128)(2,1)S(1)}, u32[]{:S(2)}, u32[]{:S(2)}) collective-permute-start(bf16[128,2048]{1,0:T(8,128)(2,1)S(1)} %collective-permute-done.20.refs_8_.refs_6_), channel_id=1, source_target_pairs={{0,8},{8,0},{16,24},{24,16},{1,9},{9,1},{17,25},{25,17},{2,10},{10... | collective-permute-start | bytes 1572872 | tf_op jit(solution)/shard_map/ppermute | solution.py:28
  124.5 23.3 %collective-permute-start.31 = (bf16[128,1024]{1,0:T(8,128)(2,1)S(1)}, bf16[128,1024]{1,0:T(8,128)(2,1)S(1)}, u32[]{:S(2)}, u32[]{:S(2)}) collective-permute-start(bf16[128,1024]{1,0:T(8,128)(2,1)S(1)} %get-tuple-element.119.refs_5_), channel_id=1, source_target_pairs={{0,8},{8,0},{16,24},{24,16},{1,9},{9,1},{17,25},{25,17},{2,10},{10... | collective-permute-start | bytes 786440 | tf_op jit(solution)/shard_map/ppermute | solution.py:28
  163.4 21.7 %collective-permute-start.27 = (bf16[256,512]{1,0:T(8,128)(2,1)S(1)}, bf16[256,512]{1,0:T(8,128)(2,1)S(1)}, u32[]{:S(2)}, u32[]{:S(2)}) collective-permute-start(bf16[256,512]{1,0:T(8,128)(2,1)S(1)} %stack_columns.3.refs_4_), channel_id=1, source_target_pairs={{0,8},{8,0},{16,24},{24,16},{1,9},{9,1},{17,25},{25,17},{2,10},{10... | collective-permute-start | bytes 786440 | tf_op jit(solution)/shard_map/ppermute | solution.py:28
  185.1 20.4 %collective-permute-start.44 = (bf16[32,1536]{1,0:T(8,128)(2,1)S(1)}, bf16[32,1536]{1,0:T(8,128)(2,1)S(1)}, u32[]{:S(2)}, u32[]{:S(2)}) collective-permute-start(bf16[32,1536]{1,0:T(8,128)(2,1)S(1)} %get-tuple-element.130), channel_id=1, source_target_pairs={{0,5},{1,4},{2,7},{3,6},{4,1},{5,0},{6,3},{7,2},{8,13},{9,12},{10,... | collective-permute-start | bytes 294920 | tf_op jit(solution)/shard_map/ppermute | solution.py:28
  (33 other events, 349.1 us)
